TPU v7x, 32 devices: a whole 2x2x4 slice. The times are simulated.
32 devices in a mesh: sp: 8 (over z, x), tp: 4 (over y, core).
Axes of the slice: x: 2, y: 2, z: 4, core: 2. Of those that a mesh axis runs over, the one named last changes fastest.
Arguments:
- queries: bfloat16 [1024, 2048], P('sp', 'tp'), may hold values from -15 to 15
- key_rows: bfloat16 [1024, 2048], P('sp', 'tp'), may hold values from -6 to 6
- value_rows: bfloat16 [1024, 2048], P('sp', 'tp'), may hold values from -6 to 6
- break_bias: bfloat16 [1024, 16], P('sp', 'tp'), may hold values from -14 to 1
- stream: bfloat16 [1024, 4096], P('sp', 'tp'), may hold values from -24 to 24
- out_proj: bfloat16 [2048, 4096], P(None, 'tp'), may hold values from -0.5 to 0.5
- norm_gain: float32 [4096], P('tp'), may hold values from 0.1 to 1.9
- expert_ids: int32 [1024, 2], P('sp'), may hold values from 0 to 15, all different within a row; in each aligned block of 128 rows (0 to 127, 128 to 255, ...) at most 32 rows name the same one
- route_weights: float32 [1024, 2], P('sp'), may hold values from 0.1 to 2.5
- gate_proj: bfloat16 [16, 4096, 384], P('sp', 'tp'), may hold values from -0.09375 to 0.09375
- up_proj: bfloat16 [16, 4096, 384], P('sp', 'tp'), may hold values from -0.09375 to 0.09375
- down_proj: bfloat16 [16, 384, 4096], P('sp', None, 'tp'), may hold values from -0.3125 to 0.3125
- shared_gate: bfloat16 [4096, 384], P('tp'), may hold values from -0.09375 to 0.09375
- shared_up: bfloat16 [4096, 384], P('tp'), may hold values from -0.09375 to 0.09375
- shared_down: bfloat16 [384, 4096], P(None, 'tp'), may hold values from -0.3125 to 0.3125
Outputs:
- result: bfloat16 [1024, 4096], P('sp', 'tp')
Inputs may be any that keep to these rules, and one draw needn't show every extreme that they name: `expert_ids`: each row names 2 different experts; within the rows of one index of sp no expert is named by more than 32 rows, a bound that some block reaches of them.
All inputs are finite; a program needn't handle non-finite values.
Results may differ from a plain program's by a relative error of at most 0.022.
Values may be sent and summed in bfloat16 or wider, within the bound.
A program may use at most 64 MiB of HBM per device.

v0:
```python
import functools

import jax
import jax.numpy as jnp
from jax import lax
from jax.experimental import pallas as pl
from jax.experimental.pallas import tpu as pltpu
from jax.sharding import PartitionSpec as P

EPS = 1e-06
F32 = jnp.float32
BF16 = jnp.bfloat16


def attention_kernel(
    heads, hd, n_sp, inner, q_ref, k_ref, v_ref, b_ref, o_ref, kbuf, vbuf, bbuf, acc, carry, send_sem, recv_sem
):
    tok = q_ref.shape[0]
    own = lax.axis_index("sp")
    outer = n_sp // inner
    z_own = own // inner
    x_own = own % inner
    above = z_own < outer - 1
    below = z_own > 0

    barrier = pltpu.get_barrier_semaphore()

    def greet(target):
        pl.semaphore_signal(
            barrier, inc=1, device_id={"sp": target}, device_id_type=pl.DeviceIdType.MESH
        )

    @pl.when(above)
    def _():
        greet(own + inner)

    @pl.when(below)
    def _():
        greet(own - inner)

    for d in range(1, inner):
        greet(z_own * inner + (x_own + d) % inner)
    pl.semaphore_wait(barrier, inner - 1 + above.astype(jnp.int32) + below.astype(jnp.int32))

    def copies(sources, block, z_block, lane, target):
        return [
            pltpu.make_async_remote_copy(
                src_ref=src,
                dst_ref=dst.at[block],
                send_sem=send_sem.at[kind, z_block, lane],
                recv_sem=recv_sem.at[kind, block],
                device_id={"sp": target},
                device_id_type=pl.DeviceIdType.MESH,
            )
            for kind, (src, dst) in enumerate(zip(sources, (kbuf, vbuf, bbuf)))
        ]

    def held(block):
        return (kbuf.at[block], vbuf.at[block], bbuf.at[block])

    def start_all(group):
        for c in group:
            c.start()

    def wait_sent(group):
        for c in group:
            c.wait_send()

    def wait_arrived(block):
        for c in copies(held(block), block, 0, 0, (own + 1) % n_sp):
            c.wait_recv()

    def own_sends(act):
        mine = (k_ref, v_ref, b_ref)

        @pl.when(above)
        def _():
            act(copies(mine, own, z_own, 0, own + inner))

        for d in range(1, inner):
            x_to = (x_own + d) % inner

            @pl.when(x_to > x_own)
            def _():
                act(copies(mine, own, z_own, d, z_own * inner + x_to))

    def relays(z_block, act):
        block = z_block * inner + x_own

        @pl.when(above)
        def _():
            act(copies(held(block), block, z_block, 0, own + inner))

        for d in range(1, inner):
            act(copies(held(block), block, z_block, d, z_own * inner + (x_own + d) % inner))

    own_sends(start_all)

    scale = hd ** (-0.5)
    row = lax.broadcasted_iota(jnp.int32, (tok, tok), 0)
    col = lax.broadcasted_iota(jnp.int32, (tok, tok), 1)
    later = (row > col).astype(F32)
    sums = jnp.concatenate([later, jnp.ones((tok, tok), F32)], axis=1).astype(BF16)
    sums = jnp.concatenate([sums, sums], axis=0)
    pick_rows = max(16, heads)
    pick = (
        lax.broadcasted_iota(jnp.int32, (pick_rows, hd), 0)
        == lax.broadcasted_iota(jnp.int32, (pick_rows, hd), 1)
    ).astype(F32).astype(BF16)
    acc[...] = jnp.zeros_like(acc)
    carry[...] = jnp.zeros_like(carry)

    def compute(keys, values, offsets, diagonal):
        bias = lax.dot_general(
            pick, offsets[...], (((1,), (1,)), ((), ())), preferred_element_type=F32
        )
        for h in range(heads):
            cols = slice(h * hd, (h + 1) * hd)
            z = lax.dot_general(
                q_ref[:, cols], keys[:, cols], (((1,), (1,)), ((), ())), preferred_element_type=F32
            )
            z = z * scale + bias[h : h + 1, :]
            low = jnp.log1p(jnp.exp(-jnp.abs(z)))
            fail = -(jnp.maximum(z, 0.0) + low)
            hit = jnp.minimum(z, 0.0) - low
            if diagonal:
                before = col < row
                fail = jnp.where(before, fail, 0.0)
            high = fail.astype(BF16)
            rest = (fail - high.astype(F32)).astype(BF16)
            both = jnp.dot(
                jnp.concatenate([high, rest], axis=1), sums, preferred_element_type=F32
            )
            before_sum = carry[h]
            w = jnp.exp(hit + both[:, :tok] + before_sum)
            if diagonal:
                w = jnp.where(before, w, 0.0)
            carry[h] = before_sum + both[:, tok:]
            acc[:, cols] += jnp.dot(w.astype(BF16), values[:, cols], preferred_element_type=F32)

    compute(k_ref, v_ref, b_ref, True)

    def group(i, _):
        z_block = z_own - i

        @pl.when(z_block > 0)
        def _():
            wait_arrived((z_block - 1) * inner + x_own)
            relays(z_block - 1, start_all)

        def member(m, _):
            x_block = inner - 1 - m
            block = z_block * inner + x_block

            @pl.when(block < own)
            def _():
                @pl.when(x_block != x_own)
                def _():
                    wait_arrived(block)

                compute(*held(block), False)

            return 0

        lax.fori_loop(0, inner, member, 0)
        return 0

    lax.fori_loop(0, z_own + 1, group, 0)
    o_ref[...] = acc[...].astype(BF16)

    own_sends(wait_sent)

    def drain(z_block, _):
        relays(z_block, wait_sent)
        return 0

    lax.fori_loop(0, z_own, drain, 0)


def attention(queries, keys, values, bias, heads, hd, n_sp):
    tok = queries.shape[0]
    inner = max(d for d in range(1, n_sp + 1) if n_sp % d == 0 and d * d <= n_sp)
    vmem = pl.BlockSpec(memory_space=pltpu.VMEM)
    return pl.pallas_call(
        functools.partial(attention_kernel, heads, hd, n_sp, inner),
        out_shape=jax.ShapeDtypeStruct((tok, heads * hd), BF16),
        in_specs=[vmem] * 4,
        out_specs=vmem,
        scratch_shapes=[
            pltpu.VMEM((n_sp, tok, heads * hd), BF16),
            pltpu.VMEM((n_sp, tok, heads * hd), BF16),
            pltpu.VMEM((n_sp, tok, hd), BF16),
            pltpu.VMEM((tok, heads * hd), F32),
            pltpu.VMEM((heads, tok, tok), F32),
            pltpu.SemaphoreType.DMA((3, n_sp // inner, inner)),
            pltpu.SemaphoreType.DMA((3, n_sp)),
        ],
        compiler_params=pltpu.CompilerParams(
            vmem_limit_bytes=40 * 2**20, collective_id=0, has_side_effects=True
        ),
        cost_estimate=pl.CostEstimate(flops=2 * 10**9, bytes_accessed=2**22, transcendentals=10**6),
    )(queries, keys, values, bias)


def exchange_kernel(n_tp, gu_ref, o_ref, parts, mine, spread, send_parts, recv_parts, send_rows, recv_rows):
    width = gu_ref.shape[2] // 2
    me = lax.axis_index("tp")
    barrier = pltpu.get_barrier_semaphore()
    others = [(me + d) % n_tp for d in range(1, n_tp)]
    for to in others:
        pl.semaphore_signal(
            barrier, inc=1, device_id={"tp": to}, device_id_type=pl.DeviceIdType.MESH
        )
    pl.semaphore_wait(barrier, n_tp - 1)
    first, second = [], []
    for d, to in enumerate(others):
        copy = pltpu.make_async_remote_copy(
            src_ref=gu_ref.at[to],
            dst_ref=parts.at[d],
            send_sem=send_parts.at[d],
            recv_sem=recv_parts.at[d],
            device_id={"tp": to},
            device_id_type=pl.DeviceIdType.MESH,
        )
        copy.start()
        first.append(copy)
    total = gu_ref[me].astype(F32)
    for d, copy in enumerate(first):
        copy.wait_recv()
        total = total + parts[d].astype(F32)
    gate = total[:, :width]
    mine[...] = (jax.nn.silu(gate) * total[:, width:]).astype(BF16)
    for d, to in enumerate(others):
        copy = pltpu.make_async_remote_copy(
            src_ref=mine,
            dst_ref=spread.at[d],
            send_sem=send_rows.at[d],
            recv_sem=recv_rows.at[d],
            device_id={"tp": to},
            device_id_type=pl.DeviceIdType.MESH,
        )
        copy.start()
        second.append(copy)
    o_ref[me] = mine[...]
    for d, copy in enumerate(second):
        copy.wait_recv()
        o_ref[(me + n_tp - 1 - d) % n_tp] = spread[d]
    for copy in first + second:
        copy.wait_send()


def exchange(gate_up, n_tp):
    rows, width = gate_up.shape[0] // n_tp, gate_up.shape[1] // 2
    vmem = pl.BlockSpec(memory_space=pltpu.VMEM)
    dma = pltpu.SemaphoreType.DMA((n_tp - 1,))
    hidden = pl.pallas_call(
        functools.partial(exchange_kernel, n_tp),
        out_shape=jax.ShapeDtypeStruct((n_tp, rows, width), BF16),
        in_specs=[vmem],
        out_specs=vmem,
        scratch_shapes=[
            pltpu.VMEM((n_tp - 1, rows, 2 * width), BF16),
            pltpu.VMEM((rows, width), BF16),
            pltpu.VMEM((n_tp - 1, rows, width), BF16),
            dma,
            dma,
            dma,
            dma,
        ],
        compiler_params=pltpu.CompilerParams(
            vmem_limit_bytes=24 * 2**20, collective_id=1, has_side_effects=True
        ),
        cost_estimate=pl.CostEstimate(flops=10**8, bytes_accessed=2**21, transcendentals=10**5),
    )(gate_up.reshape(n_tp, rows, 2 * width))
    return hidden.reshape(n_tp * rows, width)


def body(
    queries,
    key_rows,
    value_rows,
    break_bias,
    stream,
    out_proj,
    norm_gain,
    expert_ids,
    route_weights,
    gate_proj,
    up_proj,
    down_proj,
    shared_gate,
    shared_up,
    shared_down,
):
    tok = queries.shape[0]
    heads = break_bias.shape[1]
    hd = queries.shape[1] // heads
    n_sp = lax.axis_size("sp")
    n_tp = lax.axis_size("tp")
    width = stream.shape[1] * n_tp

    bias_wide = jnp.pad(break_bias, ((0, 0), (0, hd - heads)))

    experts_local = gate_proj.shape[0]
    experts = experts_local * n_sp
    top_k = expert_ids.shape[1]
    cap = 2 * top_k * tok // experts
    expert_of = jnp.arange(experts, dtype=jnp.int32)
    named = expert_ids[:, :, None] == expert_of[None, None, :]
    named_any = jnp.any(named, axis=1).astype(BF16)
    token = jnp.arange(tok, dtype=jnp.int32)
    earlier = (token[None, :] < token[:, None]).astype(BF16)
    rank_all = jnp.dot(earlier, named_any, preferred_element_type=F32)
    rank = jnp.sum(jnp.where(named, rank_all[:, None, :], 0.0), axis=2).astype(jnp.int32)
    slot = expert_ids * cap + rank
    slots = experts * cap
    place = jnp.arange(slots, dtype=jnp.int32)
    spot = slot[:, :, None] == place[None, None, :]
    send_pick = jnp.any(spot, axis=1).astype(BF16)
    back_pick = jnp.sum(jnp.where(spot, route_weights[:, :, None], 0.0), axis=1).astype(BF16)

    attended = attention(queries, key_rows, value_rows, bias_wide, heads, hd, n_sp)
    projected = jnp.dot(
        lax.all_gather(attended, "tp", axis=1, tiled=True), out_proj, preferred_element_type=F32
    )
    mixed = (stream.astype(F32) + projected).astype(BF16)
    mixed = lax.optimization_barrier(mixed)
    mixed_f = mixed.astype(F32)
    square_sum = lax.psum(jnp.sum(mixed_f * mixed_f, axis=1), "tp")
    inv_rms = lax.rsqrt(square_sum / width + EPS)
    normed = (mixed_f * inv_rms[:, None] * norm_gain[None, :]).astype(BF16)

    send = lax.dot_general(
        send_pick, normed, (((0,), (0,)), ((), ())), preferred_element_type=F32
    ).astype(BF16)
    send = send.reshape(n_sp, experts_local * cap, normed.shape[1])
    arrived = lax.all_to_all(send, "sp", split_axis=0, concat_axis=0, tiled=True)
    arrived = arrived.reshape(n_sp, experts_local, cap, -1)
    gates, ups = [], []
    for e in range(experts_local):
        rows = arrived[:, e].reshape(n_sp * cap, -1)
        gates.append(jnp.dot(rows, gate_proj[e], preferred_element_type=F32).astype(BF16))
        ups.append(jnp.dot(rows, up_proj[e], preferred_element_type=F32).astype(BF16))
    gates.append(jnp.dot(normed, shared_gate, preferred_element_type=F32).astype(BF16))
    ups.append(jnp.dot(normed, shared_up, preferred_element_type=F32).astype(BF16))
    gate_all = jnp.concatenate(gates, axis=0)
    up_all = jnp.concatenate(ups, axis=0)
    gate_up = jnp.concatenate([gate_all, up_all], axis=1)
    hidden = exchange(gate_up, n_tp)
    outs = []
    for e in range(experts_local):
        rows = hidden[e * n_sp * cap : (e + 1) * n_sp * cap]
        out = jnp.dot(rows, down_proj[e], preferred_element_type=F32).astype(BF16)
        outs.append(out.reshape(n_sp, 1, cap, -1))
    expert_out = jnp.concatenate(outs, axis=1).reshape(n_sp, experts_local * cap, -1)
    returned = lax.all_to_all(expert_out, "sp", split_axis=0, concat_axis=0, tiled=True)
    returned = returned.reshape(slots, -1)
    shared_out = jnp.dot(
        hidden[experts_local * n_sp * cap :], shared_down, preferred_element_type=F32
    )
    routed = jnp.dot(back_pick, returned, preferred_element_type=F32)
    return (mixed_f + shared_out + routed).astype(BF16)


def solution(mesh):
    in_specs = (
        P("sp", "tp"),
        P("sp", "tp"),
        P("sp", "tp"),
        P("sp", "tp"),
        P("sp", "tp"),
        P(None, "tp"),
        P("tp"),
        P("sp", None),
        P("sp", None),
        P("sp", "tp", None),
        P("sp", "tp", None),
        P("sp", None, "tp"),
        P("tp", None),
        P("tp", None),
        P(None, "tp"),
    )
    return jax.shard_map(body, mesh=mesh, in_specs=in_specs, out_specs=P("sp", "tp"), check_vma=False)
```

profile of v0, /device:TPU:0, one launch (start us, length us, event | category | flops | bytes accessed | tf_op | source)
XLA Modules:
  0.0 138.4 jit_solution(14961164337410744697)
XLA Ops:
  0.0 0.0 copy-start
  0.0 0.9 copy.28
  0.9 0.0 copy-start.1
  0.9 0.9 copy-done.1
  1.8 0.0 copy-start.2
  1.8 0.9 copy-done.2
  2.7 0.0 copy-start.3
  2.7 0.9 copy-done.3
  3.6 0.0 copy-start.4
  3.6 0.0 copy-start.5
  3.6 9.8 %shard_map.145 = bf16[128,512]{1,0:T(8,128)(2,1)S(1)} custom-call(bf16[128,512]{1,0:T(8,128)(2,1)S(1)} %copy-done.1, bf16[128,512]{1,0:T(8,128)(2,1)S(1)} %copy-done.2, bf16[128,512]{1,0:T(8,128)(2,1)S(1)} %copy-done.3, bf16[128,128]{1,0:T(8,128)(2,1)S(1)} %pad.4.b_ref), custom_call_target="tpu_custom_call" | custom-call | flops 2000000000 | bytes 4194304 | tf_op jit(solution)/shard_map/pallas_call | solution.py:184
  13.4 7.2 %all_gather.3 = bf16[128,2048]{1,0:T(8,128)(2,1)S(1)} all-gather(bf16[128,512]{1,0:T(8,128)(2,1)S(1)} %shard_map.145), channel_id=1, replica_groups=mesh['sp'=8,'tp'=4] {'tp'}, dimensions={1}, use_global_device_ids=true | all-gather | bytes 655360 | tf_op jit(solution)/shard_map/all_gather | solution.py:324
  20.6 0.0 copy-done.4
  20.6 0.0 copy-done.5
  20.6 0.0 copy-start.6
  20.6 0.0 copy-start.7
  20.6 0.8 fusion.1
  21.4 0.0 copy-start.12
  21.4 0.1 fusion.14
  21.5 6.6 %psum.7 = f32[128]{0:T(128)S(1)} all-reduce(f32[128]{0:T(128)S(1)} %fusion.14), channel_id=1, replica_groups=mesh['sp'=8,'tp'=4] {'tp'}, use_global_device_ids=true, to_apply=%region_4.5 | all-reduce | flops 128 | bytes 1024 | tf_op jit(solution)/shard_map/psum | solution.py:329
  28.1 0.0 copy-done.6
  28.1 0.1 fusion.22
  28.3 0.1 fusion.17
  28.4 0.0 copy-done.7
  28.4 1.5 %convolution_convert_fusion = bf16[512,1024]{1,0:T(8,128)(2,1)} fusion(pred[128,512]{1,0:T(8,128)(4,1)S(1)} %fusion.17, bf16[128,1024]{1,0:T(8,128)(2,1)S(1)} %fusion.1, f32[1024]{0:T(1024)S(1)} %copy-done.7, f32[128]{0:T(128)S(1)} %add_rsqrt_fusion), kind=kOutput, calls=%fused_computation | convolution fusion | flops 135266304 | bytes 1380864 | tf_op jit(solution)/shard_map/dot_general | solution.py:333
  29.9 28.4 %all-to-all-start = ((bf16[8,64,1024]{2,1,0:T(8,128)(2,1)}), bf16[8,64,1024]{2,1,0:T(8,128)(2,1)S(1)}, u32[]{:S(2)}, u32[]{:S(2)}) async-start(bf16[8,64,1024]{2,1,0:T(8,128)(2,1)} %bitcast), calls=%async_computation | async-start | bytes 2097152 | tf_op jit(solution)/shard_map/all_to_all | solution.py:337
  58.3 0.0 copy-done.12
  58.3 0.4 convolution_convert_fusion.7
  58.7 1.5 %convolution_convert_fusion.8 = bf16[128,384]{1,0:T(8,128)(2,1)S(1)} fusion(bf16[1024,384]{1,0:T(8,128)(2,1)} %param.27, bf16[128,1024]{1,0:T(8,128)(2,1)S(1)} %fusion.1, f32[1024]{0:T(1024)S(1)} %copy-done.7, f32[128]{0:T(128)S(1)} %add_rsqrt_fusion), kind=kOutput, calls=%fused_computation.13 | convolution fusion | flops 101236736 | bytes 1151488 | tf_op jit(solution)/shard_map/dot_general | solution.py:344
  60.2 23.4 %all-to-all-done = bf16[8,64,1024]{2,1,0:T(8,128)(2,1)S(1)} async-done(((bf16[8,64,1024]{2,1,0:T(8,128)(2,1)}), bf16[8,64,1024]{2,1,0:T(8,128)(2,1)S(1)}, u32[]{:S(2)}, u32[]{:S(2)}) %all-to-all-start) | async-done | bytes 1048608 | tf_op jit(solution)/shard_map/all_to_all | solution.py:337
  83.6 0.0 copy-start.9
  83.6 0.1 fusion.27
  83.7 0.0 copy-start.10
  83.7 1.3 copy-done.9
  85.0 0.4 convolution_convert_fusion.3
  85.4 0.4 convolution_convert_fusion.4
  85.9 0.0 copy-done.10
  85.9 0.4 convolution_convert_fusion.5
  86.3 0.4 convolution_convert_fusion.6
  86.8 0.0 copy-start.11
  86.8 0.1 maximum_maximum_fusion
  86.9 17.7 %shard_map.146 = bf16[4,160,384]{2,1,0:T(8,128)(2,1)S(1)} custom-call(bf16[4,160,768]{2,1,0:T(8,128)(2,1)S(1)} %bitcast.45), custom_call_target="tpu_custom_call" | custom-call | flops 100000000 | bytes 2097152 | tf_op jit(solution)/shard_map/pallas_call | solution.py:256
  104.6 0.0 copy-done.11
  104.6 0.4 convolution_convert_fusion.1
  105.0 0.4 convolution_convert_fusion.2
  105.5 0.0 copy-start.8
  105.5 1.1 pad_maximum_fusion
  106.5 3.6 %all-to-all-start.1 = ((bf16[8,64,1024]{2,1,0:T(8,128)(2,1)}), bf16[8,64,1024]{2,1,0:T(8,128)(2,1)S(1)}, u32[]{:S(2)}, u32[]{:S(2)}) async-start(bf16[8,64,1024]{2,1,0:T(8,128)(2,1)} %bitcast.16), calls=%async_computation.1 | async-start | bytes 2097152 | tf_op jit(solution)/shard_map/all_to_all | solution.py:356
  110.1 0.0 copy-done.8
  110.1 0.1 select_reduce_fusion
  110.3 0.0 copy-done
  110.3 0.3 convolution_add_fusion.2
  110.6 26.8 %all-to-all-done.1 = bf16[8,64,1024]{2,1,0:T(8,128)(2,1)S(1)} async-done(((bf16[8,64,1024]{2,1,0:T(8,128)(2,1)}), bf16[8,64,1024]{2,1,0:T(8,128)(2,1)S(1)}, u32[]{:S(2)}, u32[]{:S(2)}) %all-to-all-start.1) | async-done | bytes 1048608 | tf_op jit(solution)/shard_map/all_to_all | solution.py:356
  137.4 1.0 fusion
  (5 shorter events, 0.1 us)
Async XLA Ops:
  0.0 110.3 %copy-start = (bf16[384,1024]{1,0:T(8,128)(2,1)S(1)}, bf16[384,1024]{1,0:T(8,128)(2,1)}, u32[]{:S(2)}) copy-start(bf16[384,1024]{1,0:T(8,128)(2,1)} %param.29) | copy-start | bytes 2359300
  0.9 0.9 copy-start.1
  1.8 0.9 copy-start.2
  2.7 0.9 copy-start.3
  3.6 17.0 %copy-start.4 = (bf16[2048,1024]{1,0:T(8,128)(2,1)S(1)}, bf16[2048,1024]{1,0:T(8,128)(2,1)}, u32[]{:S(2)}) copy-start(bf16[2048,1024]{1,0:T(8,128)(2,1)} %param.20) | copy-start | bytes 12582916
  3.6 17.0 %copy-start.5 = (bf16[128,1024]{1,0:T(8,128)(2,1)S(1)}, bf16[128,1024]{1,0:T(8,128)(2,1)}, u32[]{:S(2)}) copy-start(bf16[128,1024]{1,0:T(8,128)(2,1)} %param.19) | copy-start | bytes 786436
  20.6 7.5 %copy-start.6 = (s32[128,2]{0,1:T(2,128)S(1)}, s32[128,2]{0,1:T(2,128)}, u32[]{:S(2)}) copy-start(s32[128,2]{0,1:T(2,128)} %param.22) | copy-start | bytes 3076
  20.6 7.8 %copy-start.7 = (f32[1024]{0:T(1024)S(1)}, f32[1024]{0:T(1024)}, u32[]{:S(2)}) copy-start(f32[1024]{0:T(1024)} %param.21) | copy-start | bytes 12292
  21.4 37.0 %copy-start.12 = (bf16[1024,384]{1,0:T(8,128)(2,1)S(1)}, bf16[1024,384]{1,0:T(8,128)(2,1)}, u32[]{:S(2)}) copy-start(bf16[1024,384]{1,0:T(8,128)(2,1)} %param.28) | copy-start | bytes 2359300
  29.9 53.6 %all-to-all-start = ((bf16[8,64,1024]{2,1,0:T(8,128)(2,1)}), bf16[8,64,1024]{2,1,0:T(8,128)(2,1)S(1)}, u32[]{:S(2)}, u32[]{:S(2)}) async-start(bf16[8,64,1024]{2,1,0:T(8,128)(2,1)} %bitcast), calls=%async_computation | async-start | bytes 2097152 | tf_op jit(solution)/shard_map/all_to_all | solution.py:337
  83.6 1.4 %copy-start.9 = (bf16[2,1024,384]{2,1,0:T(8,128)(2,1)S(1)}, bf16[2,1024,384]{2,1,0:T(8,128)(2,1)}, u32[]{:S(2)}) copy-start(bf16[2,1024,384]{2,1,0:T(8,128)(2,1)} %param.25) | copy-start | bytes 4718596
  83.7 2.2 %copy-start.10 = (bf16[2,1024,384]{2,1,0:T(8,128)(2,1)S(1)}, bf16[2,1024,384]{2,1,0:T(8,128)(2,1)}, u32[]{:S(2)}) copy-start(bf16[2,1024,384]{2,1,0:T(8,128)(2,1)} %param.24) | copy-start | bytes 4718596
  86.8 17.8 %copy-start.11 = (bf16[2,384,1024]{2,1,0:T(8,128)(2,1)S(1)}, bf16[2,384,1024]{2,1,0:T(8,128)(2,1)}, u32[]{:S(2)}) copy-start(bf16[2,384,1024]{2,1,0:T(8,128)(2,1)} %param.26) | copy-start | bytes 4718596
  105.5 4.7 %copy-start.8 = (f32[128,2]{0,1:T(2,128)S(1)}, f32[128,2]{0,1:T(2,128)}, u32[]{:S(2)}) copy-start(f32[128,2]{0,1:T(2,128)} %param.23) | copy-start | bytes 3076
  106.5 30.9 %all-to-all-start.1 = ((bf16[8,64,1024]{2,1,0:T(8,128)(2,1)}), bf16[8,64,1024]{2,1,0:T(8,128)(2,1)S(1)}, u32[]{:S(2)}, u32[]{:S(2)}) async-start(bf16[8,64,1024]{2,1,0:T(8,128)(2,1)} %bitcast.16), calls=%async_computation.1 | async-start | bytes 2097152 | tf_op jit(solution)/shard_map/all_to_all | solution.py:356
where the time goes:
time: 139 us; the launch traced here: 138 us
  waiting for transfers between devices  50.2 us (36%)
  starting transfers between devices  32 us (23%)
  Pallas kernels  27.4 us (20%)
  blocking collectives  13.8 us (10%)
  matrix products  8.19 us (6%)
  local copies, waits for them, and re-layouts  5.03 us (4%)
  other arithmetic  1.61 us (1%)
    all_to_all x1, starting transfers between devices, body(): lax.all_to_all(send, 'sp', split_axis=0, concat_axis=0, tiled=True)  28.4 us
    all_to_all x1, waiting for transfers between devices, body(): lax.all_to_all(expert_out, 'sp', split_axis=0, concat_axis=0, tiled=True)  26.8 us
    all_to_all x1, waiting for transfers between devices, body(): lax.all_to_all(send, 'sp', split_axis=0, concat_axis=0, tiled=True)  23.4 us
    pallas_call x1, Pallas kernels, exchange(): pl.pallas_call(functools.partial(exchange_kernel, n_tp), out_shape=jax.Sh...  17.7 us
    pallas_call x1, Pallas kernels, attention(): pl.pallas_call(functools.partial(attention_kernel, heads, hd, n_sp, inner...  9.76 us
    all_gather x1, blocking collectives, body(): lax.all_gather(attended, 'tp', axis=1, tiled=True)  7.2 us
    psum x1, blocking collectives, body(): square_sum = lax.psum(jnp.sum(mixed_f * mixed_f, axis=1), 'tp')  6.56 us
    unnamed x27, local copies, waits for them, and re-layouts  4.95 us
  transfers between devices with their start and end apart: 2, of which 2 were waited for; matrix products, arithmetic and copies ran while one was open for 2% of the time, Pallas kernels for 0%

commit v1 on v0

--- a/solution.py
+++ b/solution.py
@@ -275,6 +275,490 @@
     return hidden.reshape(n_tp * rows, width)
 
 
+MESH = pl.DeviceIdType.MESH
+
+
+def rows_contract(lhs, rhs):
+    return lax.dot_general(lhs, rhs, (((1,), (1,)), ((), ())), preferred_element_type=F32)
+
+
+def rcopy(src, dst, send_sem, recv_sem, where):
+    return pltpu.make_async_remote_copy(
+        src_ref=src,
+        dst_ref=dst,
+        send_sem=send_sem,
+        recv_sem=recv_sem,
+        device_id=where,
+        device_id_type=MESH,
+    )
+
+
+def plane_order(z, outer):
+    if outer != 4:
+        return [(z + i) % outer for i in range(outer)]
+    middle = ((z + 1) // 2) % 2
+    near = z + 1 - 2 * (z % 2)
+    across = 3 - z
+    two = (z + 2) % 4
+    return [
+        z,
+        near,
+        middle * across + (1 - middle) * two,
+        middle * two + (1 - middle) * across,
+    ]
+
+
+def greet_all(n_sp, n_tp, own, me):
+    barrier = pltpu.get_barrier_semaphore()
+    for d in range(1, n_sp):
+        pl.semaphore_signal(
+            barrier, inc=1, device_id={"sp": (own + d) % n_sp}, device_id_type=MESH
+        )
+    for d in range(1, n_tp):
+        pl.semaphore_signal(
+            barrier, inc=1, device_id={"tp": (me + d) % n_tp}, device_id_type=MESH
+        )
+    pl.semaphore_wait(barrier, n_sp + n_tp - 2)
+
+
+class Experts:
+    def __init__(self, n_sp, n_tp, inner, experts_local, cap, refs):
+        self.n_sp, self.n_tp, self.inner = n_sp, n_tp, inner
+        self.outer = n_sp // inner
+        self.el, self.cap = experts_local, cap
+        self.rw = experts_local * cap
+        self.__dict__.update(refs)
+        self.own = lax.axis_index("sp")
+        self.me = lax.axis_index("tp")
+        self.z = self.own // inner
+        self.x = self.own % inner
+        self.order = plane_order(self.z, self.outer)
+        self.tok, self.width = self.mixed.shape
+        self.ff = self.down.shape[1]
+        self.total_width = self.width * n_tp
+
+    def load_weights(self):
+        ff = self.ff
+        self.loads = [
+            pltpu.make_async_copy(src, dst, self.w_sem.at[i])
+            for i, (src, dst) in enumerate(
+                (
+                    (self.s_gate, self.wsgu.at[:, pl.ds(0, ff)]),
+                    (self.s_up, self.wsgu.at[:, pl.ds(ff, ff)]),
+                    (self.gate, self.wgu.at[:, :, pl.ds(0, ff)]),
+                    (self.up, self.wgu.at[:, :, pl.ds(ff, ff)]),
+                    (self.down, self.wd),
+                    (self.s_down, self.wsd),
+                )
+            )
+        ]
+        for load in self.loads:
+            load.start()
+
+    def meta_copies(self, ref, send, recv):
+        return [
+            rcopy(
+                ref.at[self.own],
+                ref.at[self.own],
+                send.at[d],
+                recv.at[self.own],
+                {"sp": (self.own + d) % self.n_sp},
+            )
+            for d in range(1, self.n_sp)
+        ]
+
+    def wait_table(self, ref, send, recv, block):
+        rcopy(
+            ref.at[block], ref.at[block], send.at[0], recv.at[block], {"sp": (self.own + 1) % self.n_sp}
+        ).wait_recv()
+
+    def route(self):
+        ids = self.ids[...]
+        experts = self.el * self.n_sp
+        top_k, tok = ids.shape
+        expert_of = lax.broadcasted_iota(jnp.int32, (experts, tok), 0)
+        named = [ids[k : k + 1, :] == expert_of for k in range(top_k)]
+        named_any = functools.reduce(jnp.logical_or, named).astype(F32).astype(BF16)
+        before = (
+            lax.broadcasted_iota(jnp.int32, (tok, tok), 0)
+            < lax.broadcasted_iota(jnp.int32, (tok, tok), 1)
+        ).astype(F32).astype(BF16)
+        rank = jnp.dot(named_any, before, preferred_element_type=F32)
+        self.meta[self.own] = jnp.zeros((8, tok), F32)
+        for k in range(top_k):
+            mine = jnp.sum(jnp.where(named[k], rank, 0.0), axis=0, keepdims=True)
+            slot = ids[k : k + 1, :].astype(F32) * self.cap + mine
+            self.meta[self.own, k : k + 1, :] = slot
+        self.top_k = top_k
+        self.meta_group = self.meta_copies(self.meta, self.meta_s, self.meta_r)
+        for c in self.meta_group:
+            c.start()
+
+    def slot_hits(self, block, first, count):
+        spot = (
+            lax.broadcasted_iota(jnp.int32, (count, self.tok), 0) + first
+        ).astype(F32)
+        return [self.meta[block, k : k + 1, :] == spot for k in range(self.top_k)]
+
+    def build_back(self):
+        rows = self.inner * self.rw
+        for plane in range(self.outer):
+            hits = self.slot_hits(self.own, plane * rows, rows)
+            weight = sum(
+                jnp.where(hits[k], self.wts[k : k + 1, :], 0.0) for k in range(self.top_k)
+            )
+            self.back[plane] = jnp.transpose(weight).astype(BF16)
+
+    def dense_copy(self, src, plane, step):
+        return rcopy(
+            src,
+            self.dense.at[plane],
+            self.dense_s.at[plane, (step + 1) // 2],
+            self.dense_r.at[plane],
+            {"sp": (self.z + step) * self.inner + self.x},
+        )
+
+    def spread_own(self, act):
+        for step in (1, -1):
+
+            @pl.when(self.z < self.outer - 1 if step == 1 else self.z > 0)
+            def _():
+                act(self.dense_copy(self.mixed, self.z, step))
+
+    def hand_on(self, plane, act):
+        @pl.when((plane < self.z) & (self.z < self.outer - 1))
+        def _():
+            act(self.dense_copy(self.dense.at[plane], plane, 1))
+
+        @pl.when((plane > self.z) & (self.z > 0))
+        def _():
+            act(self.dense_copy(self.dense.at[plane], plane, -1))
+
+    def take_dense(self, i):
+        plane = self.order[i]
+        rcopy(
+            self.dense.at[plane],
+            self.dense.at[plane],
+            self.dense_s.at[plane, 0],
+            self.dense_r.at[plane],
+            {"sp": (self.own + 1) % self.n_sp},
+        ).wait_recv()
+        self.hand_on(plane, lambda c: c.start())
+
+    def cross_copies(self, i):
+        return [
+            rcopy(
+                self.picked.at[i, (self.x + d) % self.inner],
+                self.rows.at[i, self.x],
+                self.x_s.at[i, d],
+                self.x_r.at[i, self.x],
+                {"sp": self.z * self.inner + (self.x + d) % self.inner},
+            )
+            for d in range(1, self.inner)
+        ]
+
+    def select(self, i):
+        block = self.order[i] * self.inner + self.x
+        if i:
+            self.wait_table(self.meta, self.meta_s, self.meta_r, block)
+        rows = self.inner * self.rw
+        hits = self.slot_hits(block, self.z * rows, rows)
+        pick = functools.reduce(jnp.logical_or, hits).astype(F32).astype(BF16)
+        source = self.dense[self.order[i]] if i else self.mixed[...]
+        got = jnp.dot(pick, source, preferred_element_type=F32).astype(BF16)
+        for p in range(self.inner):
+            self.picked[i, p] = got[p * self.rw : (p + 1) * self.rw]
+        for c in self.cross_copies(i):
+            c.start()
+        self.rows[i, self.x] = self.picked[i, self.x]
+
+    def tp_copies(self, src, dst, send, recv):
+        return [
+            rcopy(src(to), dst, send.at[d], recv.at[self.me], {"tp": to})
+            for d, to in ((d, (self.me + d) % self.n_tp) for d in range(1, self.n_tp))
+        ]
+
+    def tp_wait(self, dst, send, recv):
+        for d in range(1, self.n_tp):
+            other = (self.me + d) % self.n_tp
+            rcopy(
+                dst(other), dst(other), send.at[0], recv.at[other], {"tp": (self.me + 1) % self.n_tp}
+            ).wait_recv()
+
+    def send_squares(self):
+        wide = self.mixed[...].astype(F32)
+        column = jnp.sum(wide * wide, axis=1, keepdims=True)
+        row = jnp.transpose(jnp.broadcast_to(column, (self.tok, self.tok)))
+        self.ssq[self.me] = row[:8]
+        self.ssq_group = self.tp_copies(
+            lambda to: self.ssq.at[self.me], self.ssq.at[self.me], self.ssq_s, self.ssq_r
+        )
+        for c in self.ssq_group:
+            c.start()
+
+    def send_scales(self):
+        self.tp_wait(lambda other: self.ssq.at[other], self.ssq_s, self.ssq_r)
+        total = self.ssq[0]
+        for p in range(1, self.n_tp):
+            total = total + self.ssq[p]
+        self.inv[self.own] = lax.rsqrt(total / self.total_width + EPS)
+        self.inv_group = self.meta_copies(self.inv, self.inv_s, self.inv_r)
+        for c in self.inv_group:
+            c.start()
+
+    def send_parts(self, s, value):
+        chunk = value.shape[0] // self.n_tp
+        for p in range(self.n_tp):
+            self.gu[s, p] = value[p * chunk : (p + 1) * chunk]
+        group = self.tp_copies(
+            lambda to: self.gu.at[s, to], self.parts.at[s, self.me], self.part_s.at[s], self.part_r.at[s]
+        )
+        for c in group:
+            c.start()
+        self.part_groups[s] = group
+
+    def gate_up(self, i):
+        if i == 0:
+            self.loads[2].wait()
+            self.loads[3].wait()
+        for d in range(1, self.inner):
+            x_from = (self.x + d) % self.inner
+            rcopy(
+                self.rows.at[i, x_from],
+                self.rows.at[i, x_from],
+                self.x_s.at[i, d],
+                self.x_r.at[i, x_from],
+                {"sp": (self.own + 1) % self.n_sp},
+            ).wait_recv()
+        normed = []
+        for d in range(self.inner):
+            block = self.order[i] * self.inner + (self.x + d) % self.inner
+            if d:
+                self.wait_table(self.meta, self.meta_s, self.meta_r, block)
+            if i or d:
+                self.wait_table(self.inv, self.inv_s, self.inv_r, block)
+        for p in range(self.inner):
+            block = self.order[i] * self.inner + p
+            hits = self.slot_hits(block, self.own * self.rw, self.rw)
+            pick = functools.reduce(jnp.logical_or, hits)
+            scale = jnp.sum(
+                jnp.where(pick, self.inv[block, 0:1, :], 0.0), axis=1, keepdims=True
+            )
+            wide = self.rows[i, p].astype(F32)
+            normed.append((wide * scale * self.gain[...]).astype(BF16))
+        out = []
+        for e in range(self.el):
+            rows = jnp.concatenate(
+                [n[e * self.cap : (e + 1) * self.cap] for n in normed], axis=0
+            )
+            out.append(jnp.dot(rows, self.wgu[e], preferred_element_type=F32).astype(BF16))
+        self.send_parts(i, jnp.concatenate(out, axis=0))
+
+    def shared_gate_up(self):
+        self.loads[0].wait()
+        self.loads[1].wait()
+        scale = jnp.transpose(jnp.broadcast_to(self.inv[self.own, 0:1, :], (self.tok, self.tok)))
+        normed = (
+            self.mixed[...].astype(F32) * scale[:, 0:1] * self.gain[...]
+        ).astype(BF16)
+        value = jnp.dot(normed, self.wsgu[...], preferred_element_type=F32).astype(BF16)
+        self.send_parts(self.outer, value)
+
+    def hidden(self, s):
+        self.tp_wait(lambda other: self.parts.at[s, other], self.part_s.at[s], self.part_r.at[s])
+        total = self.gu[s, self.me].astype(F32)
+        for d in range(1, self.n_tp):
+            total = total + self.parts[s, (self.me + d) % self.n_tp].astype(F32)
+        act = jax.nn.silu(total[:, : self.ff]) * total[:, self.ff :]
+        self.hid[s, self.me] = act.astype(BF16)
+        group = self.tp_copies(
+            lambda to: self.hid.at[s, self.me], self.hid.at[s, self.me], self.hid_s.at[s], self.hid_r.at[s]
+        )
+        for c in group:
+            c.start()
+        self.hid_groups[s] = group
+
+    def all_hidden(self, s):
+        self.tp_wait(lambda other: self.hid.at[s, other], self.hid_s.at[s], self.hid_r.at[s])
+        return jnp.concatenate([self.hid[s, p] for p in range(self.n_tp)], axis=0)
+
+    def return_copies(self, i):
+        return [
+            rcopy(
+                self.outs.at[i, (self.x + d) % self.inner],
+                self.ret.at[self.own],
+                self.ret_s.at[i, d],
+                self.ret_r.at[self.own],
+                {"sp": self.order[i] * self.inner + (self.x + d) % self.inner},
+            )
+            for d in range(0 if i else 1, self.inner)
+        ]
+
+    def down_rows(self, i):
+        if i == 0:
+            self.loads[4].wait()
+        hidden = self.all_hidden(i)
+        span = self.inner * self.cap
+        for e in range(self.el):
+            out = jnp.dot(
+                hidden[e * span : (e + 1) * span], self.wd[e], preferred_element_type=F32
+            ).astype(BF16)
+            for p in range(self.inner):
+                self.outs[i, p, e * self.cap : (e + 1) * self.cap, :] = out[
+                    p * self.cap : (p + 1) * self.cap
+                ]
+        for c in self.return_copies(i):
+            c.start()
+        if i == 0:
+            self.ret[self.own] = self.outs[0, self.x]
+
+    def shared_down(self):
+        self.loads[5].wait()
+        shared = jnp.dot(
+            self.all_hidden(self.outer), self.wsd[...], preferred_element_type=F32
+        )
+        self.acc[...] = self.mixed[...].astype(F32) + shared
+
+    def collect(self, i, last=False):
+        plane = self.order[i]
+        for d in range(0 if i else 1, self.inner):
+            block = plane * self.inner + (self.x + d) % self.inner
+            rcopy(
+                self.ret.at[block],
+                self.ret.at[block],
+                self.ret_s.at[i, d],
+                self.ret_r.at[block],
+                {"sp": (self.own + 1) % self.n_sp},
+            ).wait_recv()
+        rows = jnp.concatenate(
+            [self.ret[plane * self.inner + p] for p in range(self.inner)], axis=0
+        )
+        got = jnp.dot(self.back[plane], rows, preferred_element_type=F32)
+        if last:
+            self.out[...] = (self.acc[...] + got).astype(BF16)
+        else:
+            self.acc[...] += got
+
+    def finish(self):
+        def sent(c):
+            c.wait_send()
+
+        self.spread_own(sent)
+        for i in range(1, self.outer):
+            self.hand_on(self.order[i], sent)
+        groups = [self.meta_group, self.inv_group, self.ssq_group]
+        groups += list(self.part_groups.values()) + list(self.hid_groups.values())
+        groups += [self.cross_copies(i) for i in range(self.outer)]
+        groups += [self.return_copies(i) for i in range(self.outer)]
+        for group in groups:
+            for c in group:
+                c.wait_send()
+
+    def run(self):
+        outer = self.outer
+        self.part_groups, self.hid_groups = {}, {}
+        self.spread_own(lambda c: c.start())
+        self.send_squares()
+        self.select(0)
+        self.build_back()
+        self.send_scales()
+        self.shared_gate_up()
+        self.gate_up(0)
+        for i in range(1, outer + 1):
+            if i < outer:
+                self.take_dense(i)
+                self.select(i)
+            if i == 1:
+                self.hidden(outer)
+            self.hidden(i - 1)
+            if i == 1:
+                self.shared_down()
+            if i < outer:
+                self.gate_up(i)
+            self.down_rows(i - 1)
+        for i in range(outer):
+            self.collect(i, i == outer - 1)
+        self.finish()
+
+
+MOE_INPUTS = (
+    "mixed", "ids", "wts", "gain", "gate", "up", "down", "s_gate", "s_up", "s_down",
+)
+
+
+def moe_scratch(n_sp, n_tp, inner, el, cap, tok, width, ff):
+    outer, rw = n_sp // inner, el * cap
+    chunk = inner * rw // n_tp
+    chunk_s = tok // n_tp
+    assert chunk == chunk_s
+    vmem, dma = pltpu.VMEM, pltpu.SemaphoreType.DMA
+    return {
+        "wgu": vmem((el, width, 2 * ff), BF16),
+        "wd": vmem((el, ff, width), BF16),
+        "wsgu": vmem((width, 2 * ff), BF16),
+        "wsd": vmem((ff, width), BF16),
+        "dense": vmem((outer, tok, width), BF16),
+        "picked": vmem((outer, inner, rw, width), BF16),
+        "rows": vmem((outer, inner, rw, width), BF16),
+        "meta": vmem((n_sp, 8, tok), F32),
+        "inv": vmem((n_sp, 8, tok), F32),
+        "ssq": vmem((n_tp, 8, tok), F32),
+        "gu": vmem((outer + 1, n_tp, chunk, 2 * ff), BF16),
+        "parts": vmem((outer + 1, n_tp, chunk, 2 * ff), BF16),
+        "hid": vmem((outer + 1, n_tp, chunk, ff), BF16),
+        "outs": vmem((outer, inner, rw, width), BF16),
+        "ret": vmem((n_sp, rw, width), BF16),
+        "back": vmem((outer, tok, inner * rw), BF16),
+        "acc": vmem((tok, width), F32),
+        "w_sem": dma((6,)),
+        "meta_s": dma((n_sp,)),
+        "meta_r": dma((n_sp,)),
+        "inv_s": dma((n_sp,)),
+        "inv_r": dma((n_sp,)),
+        "ssq_s": dma((n_tp,)),
+        "ssq_r": dma((n_tp,)),
+        "dense_s": dma((outer, 2)),
+        "dense_r": dma((outer,)),
+        "x_s": dma((outer, inner)),
+        "x_r": dma((outer, inner)),
+        "part_s": dma((outer + 1, n_tp)),
+        "part_r": dma((outer + 1, n_tp)),
+        "hid_s": dma((outer + 1, n_tp)),
+        "hid_r": dma((outer + 1, n_tp)),
+        "ret_s": dma((outer, inner)),
+        "ret_r": dma((n_sp,)),
+    }
+
+
+def moe_kernel(n_sp, n_tp, inner, el, cap, names, *refs):
+    work = Experts(n_sp, n_tp, inner, el, cap, dict(zip(names, refs)))
+    work.load_weights()
+    work.route_ready = None
+    greet_all(n_sp, n_tp, work.own, work.me)
+    work.route()
+    work.run()
+
+
+def moe(mixed, ids, wts, gain, gate, up, down, s_gate, s_up, s_down, n_sp, n_tp, inner, cap):
+    tok, width = mixed.shape
+    el, ff = down.shape[:2]
+    scratch = moe_scratch(n_sp, n_tp, inner, el, cap, tok, width, ff)
+    vmem = pl.BlockSpec(memory_space=pltpu.VMEM)
+    hbm = pl.BlockSpec(memory_space=pltpu.MemorySpace.HBM)
+    names = MOE_INPUTS + ("out",) + tuple(scratch)
+    return pl.pallas_call(
+        functools.partial(moe_kernel, n_sp, n_tp, inner, el, cap, names),
+        out_shape=jax.ShapeDtypeStruct((tok, width), BF16),
+        in_specs=[vmem] * 4 + [hbm] * 6,
+        out_specs=vmem,
+        scratch_shapes=list(scratch.values()),
+        compiler_params=pltpu.CompilerParams(
+            vmem_limit_bytes=40 * 2**20, collective_id=2, has_side_effects=True
+        ),
+        cost_estimate=pl.CostEstimate(flops=10**10, bytes_accessed=2**23, transcendentals=10**6),
+    )(mixed, ids, wts, gain, gate, up, down, s_gate, s_up, s_down)
+
+
 def body(
     queries,
     key_rows,
@@ -305,6 +789,18 @@
     experts = experts_local * n_sp
     top_k = expert_ids.shape[1]
     cap = 2 * top_k * tok // experts
+    n_inner = max(d for d in range(1, n_sp + 1) if n_sp % d == 0 and d * d <= n_sp)
+    plane_rows = n_inner * experts_local * cap
+    if cap % 16 == 0 and plane_rows == tok and tok % (16 * n_tp) == 0:
+        attended = attention(queries, key_rows, value_rows, bias_wide, heads, hd, n_sp)
+        projected = jnp.dot(
+            lax.all_gather(attended, "tp", axis=1, tiled=True), out_proj, preferred_element_type=F32
+        )
+        mixed = (stream.astype(F32) + projected).astype(BF16)
+        return moe(
+            mixed, expert_ids.T, route_weights.T, norm_gain[None, :], gate_proj, up_proj, down_proj,
+            shared_gate, shared_up, shared_down, n_sp, n_tp, n_inner, cap,
+        )
     expert_of = jnp.arange(experts, dtype=jnp.int32)
     named = expert_ids[:, :, None] == expert_of[None, None, :]
     named_any = jnp.any(named, axis=1).astype(BF16)

time: 139 us -> 107 us (0.77)
  Pallas kernels: 27.4 us -> 94.1 us
  waiting for transfers between devices: 50.2 us -> 0 us
  starting transfers between devices: 32 us -> 0 us
  matrix products: 8.19 us -> 0.75 us
  blocking collectives: 13.8 us -> 7.33 us
  other arithmetic: 1.61 us -> 0 us
    pallas_call x1, Pallas kernels: 17.7 us -> 84.2 us  [moe(): pl.pallas_call(functools.partial(moe_kernel, n_sp, n_tp, inner, el, cap,...]
    all_to_all x2 -> x0, waiting for transfers between devices: 50.2 us -> none  [the longest x1 26.8 us: body(): lax.all_to_all(expert_out, 'sp', split_axis=0, concat_axis=0, tiled=True)]
    all_to_all x2 -> x0, starting transfers between devices: 32 us -> none  [the longest x1 28.4 us: body(): lax.all_to_all(send, 'sp', split_axis=0, concat_axis=0, tiled=True)]
    dot_general x12 -> x0, matrix products: 7.43 us -> none  [the longest x1 1.51 us: body(): lax.dot_general(send_pick, normed, (((0,), (0,)), ((), ())), preferred_el...]
    psum x1 -> x0, blocking collectives: 6.56 us -> none  [body(): square_sum = lax.psum(jnp.sum(mixed_f * mixed_f, axis=1), 'tp')]
    unnamed x27 -> x30, local copies, waits for them, and re-layouts: 4.95 us -> 4.28 us
  transfers between devices with their start and end apart: 2 -> 0, of which waited for: 2 -> 0; matrix products, arithmetic and copies ran while one was open for 2% -> 0% of each run, Pallas kernels for 0% -> 0%
where the time goes in v1:
time: 107 us
  Pallas kernels  94.1 us (88%)
  blocking collectives  7.33 us (7%)
  local copies, waits for them, and re-layouts  4.29 us (4%)
    pallas_call x1, Pallas kernels, moe(): pl.pallas_call(functools.partial(moe_kernel, n_sp, n_tp, inner, el, cap,...  84.2 us
    pallas_call x1, Pallas kernels, attention(): pl.pallas_call(functools.partial(attention_kernel, heads, hd, n_sp, inner...  9.82 us
    all_gather x1, blocking collectives, body(): lax.all_gather(attended, 'tp', axis=1, tiled=True)  7.33 us
    unnamed x30, local copies, waits for them, and re-layouts  4.28 us

profile of v1, /device:TPU:0, one launch (start us, length us, event | category | flops | bytes accessed | tf_op | source)
XLA Modules:
  0.0 106.6 jit_solution(1877813373783969185)
XLA Ops:
  0.0 0.8 copy.16
  0.8 0.0 copy-start.6
  0.8 0.9 copy-done.6
  1.7 0.0 copy-start.7
  1.7 0.9 copy-done.7
  2.6 0.0 copy-start.8
  2.6 0.9 copy-done.8
  3.5 0.0 copy-start.12
  3.5 0.0 copy-start.13
  3.5 0.0 copy-start.4
  3.5 0.0 copy-start.5
  3.6 9.8 %shard_map.145 = bf16[128,512]{1,0:T(8,128)(2,1)S(1)} custom-call(bf16[128,512]{1,0:T(8,128)(2,1)S(1)} %copy-done.6, bf16[128,512]{1,0:T(8,128)(2,1)S(1)} %copy-done.7, bf16[128,512]{1,0:T(8,128)(2,1)S(1)} %copy-done.8, bf16[128,128]{1,0:T(8,128)(2,1)S(1)} %pad.4.b_ref), custom_call_target="tpu_custom_call" | custom-call | flops 2000000000 | bytes 4194304 | tf_op jit(solution)/shard_map/pallas_call | solution.py:184
  13.4 0.0 copy-start
  13.4 0.0 copy-start.1
  13.4 0.0 copy-start.2
  13.4 0.0 copy-start.3
  13.4 0.0 copy-start.9
  13.4 0.0 copy-start.10
  13.4 0.0 copy-start.11
  13.5 7.3 %all_gather.3 = bf16[128,2048]{1,0:T(8,128)(2,1)S(1)} all-gather(bf16[128,512]{1,0:T(8,128)(2,1)S(1)} %shard_map.145), channel_id=1, replica_groups=mesh['sp'=8,'tp'=4] {'tp'}, dimensions={1}, use_global_device_ids=true | all-gather | bytes 655360 | tf_op jit(solution)/shard_map/all_gather | solution.py:797
  20.8 0.0 copy-done.12
  20.8 0.0 copy-done.13
  20.8 0.8 fusion.refs_0_
  21.6 0.0 copy-done.4
  21.6 0.0 copy-done.5
  21.6 0.0 copy-done
  21.6 0.0 copy-done.1
  21.6 0.0 copy-done.2
  21.6 0.0 copy-done.3
  21.6 0.0 copy-done.9
  21.6 0.0 copy-done.10
  21.6 0.0 copy-done.11
  21.6 84.2 %shard_map.146 = bf16[128,1024]{1,0:T(8,128)(2,1)S(1)} custom-call(bf16[128,1024]{1,0:T(8,128)(2,1)S(1)} %fusion.refs_0_, s32[2,128]{1,0:T(2,128)S(1)} %bitcast.6, f32[2,128]{1,0:T(2,128)S(1)} %bitcast.7, f32[1,1024]{1,0:T(1,128)S(1)} %bitcast.5, bf16[2,1024,384]{2,1,0:T(8,128)(2,1)S(1)} %copy-done, bf16[2,1024,384]{2,1,0:T(8,128)(2,1)S(1)} %copy-done.1, ...), custom_call_target="tpu_custom_call" | custom-call | flops 10000000000 | bytes 8388608 | tf_op jit(solution)/shard_map/pallas_call | solution.py:749
  105.9 0.7 copy.18
  (1 shorter events, 0.0 us)
Async XLA Ops:
  0.8 0.9 copy-start.6
  1.7 0.9 copy-start.7
  2.6 0.9 copy-start.8
  3.5 17.3 %copy-start.12 = (bf16[2048,1024]{1,0:T(8,128)(2,1)S(1)}, bf16[2048,1024]{1,0:T(8,128)(2,1)}, u32[]{:S(2)}) copy-start(bf16[2048,1024]{1,0:T(8,128)(2,1)} %param.20) | copy-start | bytes 12582916
  3.5 17.3 %copy-start.13 = (bf16[128,1024]{1,0:T(8,128)(2,1)S(1)}, bf16[128,1024]{1,0:T(8,128)(2,1)}, u32[]{:S(2)}) copy-start(bf16[128,1024]{1,0:T(8,128)(2,1)} %param.19) | copy-start | bytes 786436
  3.5 18.0 %copy-start.4 = (bf16[1024,384]{1,0:T(8,128)(2,1)S(1)}, bf16[1024,384]{1,0:T(8,128)(2,1)}, u32[]{:S(2)}) copy-start(bf16[1024,384]{1,0:T(8,128)(2,1)} %refs_8_.1) | copy-start | bytes 2359300
  3.5 18.0 %copy-start.5 = (bf16[384,1024]{1,0:T(8,128)(2,1)S(1)}, bf16[384,1024]{1,0:T(8,128)(2,1)}, u32[]{:S(2)}) copy-start(bf16[384,1024]{1,0:T(8,128)(2,1)} %refs_9_.1) | copy-start | bytes 2359300
  13.4 8.2 %copy-start = (bf16[2,1024,384]{2,1,0:T(8,128)(2,1)S(1)}, bf16[2,1024,384]{2,1,0:T(8,128)(2,1)}, u32[]{:S(2)}) copy-start(bf16[2,1024,384]{2,1,0:T(8,128)(2,1)} %refs_4_.1) | copy-start | bytes 4718596
  13.4 8.2 %copy-start.1 = (bf16[2,1024,384]{2,1,0:T(8,128)(2,1)S(1)}, bf16[2,1024,384]{2,1,0:T(8,128)(2,1)}, u32[]{:S(2)}) copy-start(bf16[2,1024,384]{2,1,0:T(8,128)(2,1)} %refs_5_.1) | copy-start | bytes 4718596
  13.4 8.2 %copy-start.2 = (bf16[2,384,1024]{2,1,0:T(8,128)(2,1)S(1)}, bf16[2,384,1024]{2,1,0:T(8,128)(2,1)}, u32[]{:S(2)}) copy-start(bf16[2,384,1024]{2,1,0:T(8,128)(2,1)} %refs_6_.1) | copy-start | bytes 4718596
  13.4 8.2 %copy-start.3 = (bf16[1024,384]{1,0:T(8,128)(2,1)S(1)}, bf16[1024,384]{1,0:T(8,128)(2,1)}, u32[]{:S(2)}) copy-start(bf16[1024,384]{1,0:T(8,128)(2,1)} %refs_7_.1) | copy-start | bytes 2359300
  13.4 8.2 %copy-start.9 = (f32[1024]{0:T(1024)S(1)}, f32[1024]{0:T(1024)}, u32[]{:S(2)}) copy-start(f32[1024]{0:T(1024)} %param.21) | copy-start | bytes 12292
  13.4 8.2 %copy-start.10 = (s32[128,2]{0,1:T(2,128)S(1)}, s32[128,2]{0,1:T(2,128)}, u32[]{:S(2)}) copy-start(s32[128,2]{0,1:T(2,128)} %param.22) | copy-start | bytes 3076
  13.4 8.2 %copy-start.11 = (f32[128,2]{0,1:T(2,128)S(1)}, f32[128,2]{0,1:T(2,128)}, u32[]{:S(2)}) copy-start(f32[128,2]{0,1:T(2,128)} %param.23) | copy-start | bytes 3076

commit v2 on v1

--- a/solution.py
+++ b/solution.py
@@ -660,7 +660,6 @@
         self.spread_own(lambda c: c.start())
         self.send_squares()
         self.select(0)
-        self.build_back()
         self.send_scales()
         self.shared_gate_up()
         self.gate_up(0)
@@ -679,11 +678,6 @@
         for i in range(outer):
             self.collect(i, i == outer - 1)
         self.finish()
-
-
-MOE_INPUTS = (
-    "mixed", "ids", "wts", "gain", "gate", "up", "down", "s_gate", "s_up", "s_down",
-)
 
 
 def moe_scratch(n_sp, n_tp, inner, el, cap, tok, width, ff):
@@ -730,33 +724,350 @@
     }
 
 
-def moe_kernel(n_sp, n_tp, inner, el, cap, names, *refs):
-    work = Experts(n_sp, n_tp, inner, el, cap, dict(zip(names, refs)))
-    work.load_weights()
-    work.route_ready = None
-    greet_all(n_sp, n_tp, work.own, work.me)
-    work.route()
-    work.run()
-
-
-def moe(mixed, ids, wts, gain, gate, up, down, s_gate, s_up, s_down, n_sp, n_tp, inner, cap):
-    tok, width = mixed.shape
-    el, ff = down.shape[:2]
-    scratch = moe_scratch(n_sp, n_tp, inner, el, cap, tok, width, ff)
-    vmem = pl.BlockSpec(memory_space=pltpu.VMEM)
+class Attend:
+    def __init__(self, n_sp, n_tp, inner, refs):
+        self.n_sp, self.n_tp, self.inner = n_sp, n_tp, inner
+        self.outer = n_sp // inner
+        self.__dict__.update(refs)
+        self.own = lax.axis_index("sp")
+        self.me = lax.axis_index("tp")
+        self.z = self.own // inner
+        self.x = self.own % inner
+        self.order = plane_order(self.z, self.outer)
+        self.heads, self.tok = self.bias.shape
+        self.hd = self.queries.shape[1] // self.heads
+        self.partner = self.me + 1 - 2 * (self.me % 2)
+        self.peers = [(self.me + 2 * d) % n_tp for d in range(1, n_tp // 2)]
+
+    def load(self):
+        pairs = (
+            (self.keys, self.kv),
+            (self.values, self.vv),
+            (self.queries, self.qv),
+            (self.bias, self.bv),
+        )
+        self.loads = [
+            pltpu.make_async_copy(src, dst, self.a_sem.at[i]) for i, (src, dst) in enumerate(pairs)
+        ]
+        for c in self.loads:
+            c.start()
+
+    def load_late(self):
+        pairs = ((self.stream, self.sv), (self.out_proj, self.wo))
+        self.late = [
+            pltpu.make_async_copy(src, dst, self.a_sem.at[4 + i])
+            for i, (src, dst) in enumerate(pairs)
+        ]
+        for c in self.late:
+            c.start()
+
+    def head_of(self, ref, head):
+        return ref.at[:, pl.ds(pl.multiple_of(head * self.hd, self.hd), self.hd)]
+
+    def exchange_copies(self, kind, i):
+        src, dst = ((self.kv, self.kb), (self.vv, self.vb), (self.qv, self.qb))[kind]
+        plane = self.order[i]
+        target = dst.at[self.z, self.x] if kind < 2 else dst.at[self.z]
+        return [
+            rcopy(
+                self.head_of(src, plane),
+                target,
+                self.e_s.at[kind, i],
+                self.q_r.at[self.z] if kind == 2 else self.kv_r.at[kind, self.z, self.x],
+                {"sp": plane * self.inner + self.x},
+            )
+        ]
+
+    def side_copies(self, kind, i):
+        dst = (self.kb, self.vb)[kind]
+        plane = self.order[i]
+        src = dst.at[plane, self.x] if i else self.head_of((self.kv, self.vv)[kind], self.z)
+        return [
+            rcopy(
+                src,
+                dst.at[plane, self.x],
+                self.side_s.at[kind, i, d],
+                self.kv_r.at[kind, plane, self.x],
+                {"sp": self.z * self.inner + (self.x + d) % self.inner},
+            )
+            for d in range(1, self.inner)
+        ]
+
+    def wait_kv(self, kind, plane, x):
+        dst = (self.kb, self.vb)[kind].at[plane, x]
+        rcopy(
+            dst, dst, self.e_s.at[kind, 0], self.kv_r.at[kind, plane, x], {"sp": (self.own + 1) % self.n_sp}
+        ).wait_recv()
+
+    def bias_copies(self):
+        return [
+            rcopy(
+                self.bi.at[self.own],
+                self.bi.at[self.own],
+                self.bi_s.at[d],
+                self.bi_r.at[self.own],
+                {"sp": (self.own + d) % self.n_sp},
+            )
+            for d in range(1, self.n_sp)
+        ]
+
+    def exchange(self):
+        for kind in range(3):
+            self.loads[kind].wait()
+            for i in range(self.outer - 1, 0, -1):
+                for c in self.exchange_copies(kind, i):
+                    c.start()
+            if kind < 2:
+                for c in self.side_copies(kind, 0):
+                    c.start()
+        self.loads[3].wait()
+        self.bi[self.own, : self.heads, :] = self.bv[...].astype(F32)
+        for c in self.bias_copies():
+            c.start()
+        self.kb[self.z, self.x] = self.head_of(self.kv, self.z)[...]
+        self.vb[self.z, self.x] = self.head_of(self.vv, self.z)[...]
+        self.qb[self.z] = self.head_of(self.qv, self.z)[...]
+
+    def hand_over(self):
+        for i in range(1, self.outer):
+            for kind in range(2):
+                self.wait_kv(kind, self.order[i], self.x)
+                for c in self.side_copies(kind, i):
+                    c.start()
+        for d in range(1, self.n_sp):
+            block = (self.own + d) % self.n_sp
+            rcopy(
+                self.bi.at[block],
+                self.bi.at[block],
+                self.bi_s.at[d],
+                self.bi_r.at[block],
+                {"sp": (self.own + 1) % self.n_sp},
+            ).wait_recv()
+
+    def compute(self):
+        tok, hd = self.tok, self.hd
+        scale = hd ** (-0.5)
+        row = lax.broadcasted_iota(jnp.int32, (tok, tok), 0)
+        col = lax.broadcasted_iota(jnp.int32, (tok, tok), 1)
+        later = (row > col).astype(F32)
+        sums = jnp.concatenate([later, jnp.ones((tok, tok), F32)], axis=1).astype(BF16)
+        sums = jnp.concatenate([sums, sums], axis=0)
+        for j in range(self.outer):
+            for d in range(1, self.inner):
+                for kind in range(2):
+                    self.wait_kv(kind, j, (self.x + d) % self.inner)
+
+            @pl.when(self.z != j)
+            def _():
+                rcopy(
+                    self.qb.at[j], self.qb.at[j], self.e_s.at[2, 0], self.q_r.at[j], {"sp": (self.own + 1) % self.n_sp}
+                ).wait_recv()
+
+            q = self.qb[j]
+            acc = jnp.zeros((tok, hd), F32)
+            carry = jnp.zeros((tok, tok), F32)
+            for k in range(j, -1, -1):
+                for p in range(self.inner - 1, -1, -1):
+                    bias = self.bi[k * self.inner + p, pl.ds(self.z, 1), :]
+                    logit = rows_contract(q, self.kb[k, p]) * scale + bias
+                    low = jnp.log(1.0 + jnp.exp(-jnp.abs(logit)))
+                    fail = -(jnp.maximum(logit, 0.0) + low)
+                    hit = jnp.minimum(logit, 0.0) - low
+                    if k == j:
+                        before = col < row + (self.x - p) * tok
+                        fail = jnp.where(before, fail, 0.0)
+                    high = fail.astype(BF16)
+                    rest = (fail - high.astype(F32)).astype(BF16)
+                    both = jnp.dot(
+                        jnp.concatenate([high, rest], axis=1), sums, preferred_element_type=F32
+                    )
+                    w = jnp.exp(hit + both[:, :tok] + carry)
+                    if k == j:
+                        w = jnp.where(before, w, 0.0)
+                    carry = carry + both[:, tok:]
+                    acc = acc + jnp.dot(
+                        w.astype(BF16), self.vb[k, p], preferred_element_type=F32
+                    )
+            self.ob[j] = acc.astype(BF16)
+
+            @pl.when(self.z != j)
+            def _():
+                self.out_copy(j).start()
+
+            @pl.when(self.z == j)
+            def _():
+                self.att[self.me, self.z] = self.ob[j]
+
+    def out_copy(self, j):
+        return rcopy(
+            self.ob.at[j],
+            self.att.at[self.me, self.z],
+            self.o_s.at[j],
+            self.att_r.at[self.me, self.z],
+            {"sp": j * self.inner + self.x},
+        )
+
+    def wait_att(self, source, head):
+        piece = self.att.at[source, head]
+        rcopy(
+            piece, piece, self.o_s.at[0], self.att_r.at[source, head], {"tp": (self.me + 1) % self.n_tp}
+        ).wait_recv()
+
+    def piece_copies(self, source, head, slot, targets):
+        piece = self.att.at[source, head]
+        return [
+            rcopy(piece, piece, self.g_s.at[slot + n, head], self.att_r.at[source, head], {"tp": to})
+            for n, to in enumerate(targets)
+        ]
+
+    def gather(self):
+        wide = self.heads * self.hd
+
+        def part(source):
+            rows = jnp.concatenate([self.att[source, h] for h in range(self.outer)], axis=1)
+            first = pl.multiple_of(source * wide, wide)
+            return jnp.dot(rows, self.wo[pl.ds(first, wide), :], preferred_element_type=F32)
+
+        slots = 1 + len(self.peers)
+        for i in range(self.outer):
+            head = self.order[i]
+            if i:
+                self.wait_att(self.me, head)
+            for c in self.piece_copies(self.me, head, 0, self.peers + [self.partner]):
+                c.start()
+        for c in self.late:
+            c.wait()
+        self.acc[...] = self.sv[...].astype(F32) + part(self.me)
+        for n, peer in enumerate(self.peers):
+            for i in range(self.outer):
+                self.wait_att(peer, self.order[i])
+                for c in self.piece_copies(peer, self.order[i], slots + n, [self.partner]):
+                    c.start()
+        for i in range(self.outer):
+            self.wait_att(self.partner, self.order[i])
+        self.acc[...] += part(self.partner)
+        for peer in self.peers:
+            self.acc[...] += part(peer)
+        others = [(self.partner + 2 * d) % self.n_tp for d in range(1, self.n_tp // 2)]
+        for other in others:
+            for i in range(self.outer):
+                self.wait_att(other, self.order[i])
+        total = self.acc[...]
+        for other in others:
+            total = total + part(other)
+        self.mixed[...] = total.astype(BF16)
+
+    def finish(self):
+        groups = [self.bias_copies()]
+        for i in range(1, self.outer):
+            groups += [self.exchange_copies(kind, i) for kind in range(3)]
+        for i in range(self.outer):
+            groups += [self.side_copies(kind, i) for kind in range(2)]
+            groups.append(
+                self.piece_copies(self.me, self.order[i], 0, self.peers + [self.partner])
+            )
+            for n, peer in enumerate(self.peers):
+                groups.append(
+                    self.piece_copies(
+                        peer, self.order[i], 1 + len(self.peers) + n, [self.partner]
+                    )
+                )
+        for group in groups:
+            for c in group:
+                c.wait_send()
+        for j in range(self.outer):
+
+            @pl.when(self.z != j)
+            def _():
+                self.out_copy(j).wait_send()
+
+
+LAYER_INPUTS = (
+    "queries", "keys", "values", "bias", "stream", "out_proj", "gain_in", "ids_in", "wts_in",
+    "gate", "up", "down", "s_gate", "s_up", "s_down",
+)
+
+
+def attend_scratch(n_sp, n_tp, inner, heads, hd, tok, width, top_k):
+    outer = n_sp // inner
+    vmem, dma = pltpu.VMEM, pltpu.SemaphoreType.DMA
+    wide = heads * hd
+    return {
+        "qv": vmem((tok, wide), BF16),
+        "kv": vmem((tok, wide), BF16),
+        "vv": vmem((tok, wide), BF16),
+        "bv": vmem((heads, tok), BF16),
+        "sv": vmem((tok, width), BF16),
+        "wo": vmem((n_tp * wide, width), BF16),
+        "qb": vmem((outer, tok, hd), BF16),
+        "kb": vmem((outer, inner, tok, hd), BF16),
+        "vb": vmem((outer, inner, tok, hd), BF16),
+        "bi": vmem((n_sp, 8, tok), F32),
+        "ob": vmem((outer, tok, hd), BF16),
+        "att": vmem((n_tp, outer, tok, hd), BF16),
+        "mixed": vmem((tok, width), BF16),
+        "gain": vmem((1, width), F32),
+        "ids": vmem((top_k, tok), jnp.int32),
+        "wts": vmem((top_k, tok), F32),
+        "a_sem": dma((6,)),
+        "s_sem": dma((3,)),
+        "e_s": dma((3, outer)),
+        "q_r": dma((outer,)),
+        "kv_r": dma((2, outer, inner)),
+        "side_s": dma((2, outer, inner)),
+        "bi_s": dma((n_sp,)),
+        "bi_r": dma((n_sp,)),
+        "o_s": dma((outer,)),
+        "att_r": dma((n_tp, outer)),
+        "g_s": dma((n_tp, outer)),
+    }
+
+
+def layer_kernel(n_sp, n_tp, inner, el, cap, names, *refs):
+    named = dict(zip(names, refs))
+    first = Attend(n_sp, n_tp, inner, named)
+    second = Experts(n_sp, n_tp, inner, el, cap, named)
+    first.load()
+    small = [
+        pltpu.make_async_copy(named[name + "_in"], named[name], named["s_sem"].at[i])
+        for i, name in enumerate(("ids", "wts", "gain"))
+    ]
+    for c in small:
+        c.start()
+    greet_all(n_sp, n_tp, first.own, first.me)
+    first.exchange()
+    first.load_late()
+    second.load_weights()
+    for c in small:
+        c.wait()
+    second.route()
+    second.build_back()
+    first.hand_over()
+    first.compute()
+    first.gather()
+    second.run()
+    first.finish()
+
+
+def layer(operands, n_sp, n_tp, inner, cap, heads, hd):
+    tok, width = operands[4].shape
+    el, ff = operands[11].shape[:2]
+    top_k = operands[7].shape[0]
+    scratch = attend_scratch(n_sp, n_tp, inner, heads, hd, tok, width, top_k)
+    scratch |= moe_scratch(n_sp, n_tp, inner, el, cap, tok, width, ff)
     hbm = pl.BlockSpec(memory_space=pltpu.MemorySpace.HBM)
-    names = MOE_INPUTS + ("out",) + tuple(scratch)
+    names = LAYER_INPUTS + ("out",) + tuple(scratch)
     return pl.pallas_call(
-        functools.partial(moe_kernel, n_sp, n_tp, inner, el, cap, names),
+        functools.partial(layer_kernel, n_sp, n_tp, inner, el, cap, names),
         out_shape=jax.ShapeDtypeStruct((tok, width), BF16),
-        in_specs=[vmem] * 4 + [hbm] * 6,
-        out_specs=vmem,
+        in_specs=[hbm] * len(operands),
+        out_specs=pl.BlockSpec(memory_space=pltpu.VMEM),
         scratch_shapes=list(scratch.values()),
         compiler_params=pltpu.CompilerParams(
-            vmem_limit_bytes=40 * 2**20, collective_id=2, has_side_effects=True
+            vmem_limit_bytes=56 * 2**20, collective_id=0, has_side_effects=True
         ),
-        cost_estimate=pl.CostEstimate(flops=10**10, bytes_accessed=2**23, transcendentals=10**6),
-    )(mixed, ids, wts, gain, gate, up, down, s_gate, s_up, s_down)
+        cost_estimate=pl.CostEstimate(flops=10**10, bytes_accessed=2**24, transcendentals=10**6),
+    )(*operands)
 
 
 def body(
@@ -791,16 +1102,13 @@
     cap = 2 * top_k * tok // experts
     n_inner = max(d for d in range(1, n_sp + 1) if n_sp % d == 0 and d * d <= n_sp)
     plane_rows = n_inner * experts_local * cap
-    if cap % 16 == 0 and plane_rows == tok and tok % (16 * n_tp) == 0:
-        attended = attention(queries, key_rows, value_rows, bias_wide, heads, hd, n_sp)
-        projected = jnp.dot(
-            lax.all_gather(attended, "tp", axis=1, tiled=True), out_proj, preferred_element_type=F32
-        )
-        mixed = (stream.astype(F32) + projected).astype(BF16)
-        return moe(
-            mixed, expert_ids.T, route_weights.T, norm_gain[None, :], gate_proj, up_proj, down_proj,
-            shared_gate, shared_up, shared_down, n_sp, n_tp, n_inner, cap,
-        )
+    if heads * n_inner == n_sp and plane_rows == tok and cap % 16 == 0 and tok % (16 * n_tp) == 0:
+        operands = (
+            queries, key_rows, value_rows, break_bias.T, stream, out_proj, norm_gain[None, :],
+            expert_ids.T, route_weights.T, gate_proj, up_proj, down_proj,
+            shared_gate, shared_up, shared_down,
+        )
+        return layer(operands, n_sp, n_tp, n_inner, cap, heads, hd)
     expert_of = jnp.arange(experts, dtype=jnp.int32)
     named = expert_ids[:, :, None] == expert_of[None, None, :]
     named_any = jnp.any(named, axis=1).astype(BF16)

time: 107 us -> 91.8 us (0.86)
  blocking collectives: 7.33 us -> 0 us
  Pallas kernels: 94.1 us -> 90 us
  local copies, waits for them, and re-layouts: 4.29 us -> 1.67 us
    all_gather x1 -> x0, blocking collectives: 7.33 us -> none  [body(): lax.all_gather(attended, 'tp', axis=1, tiled=True)]
    pallas_call x2 -> x1, Pallas kernels: 94.1 us -> 90 us  [layer(): pl.pallas_call(functools.partial(layer_kernel, n_sp, n_tp, inner, el, cap...]
    unnamed x30 -> x1, local copies, waits for them, and re-layouts: 4.28 us -> 1.67 us
where the time goes in v2:
time: 91.8 us; the launch traced here: 91.7 us
  Pallas kernels  90 us (98%)
  local copies, waits for them, and re-layouts  1.67 us (2%)
    pallas_call x1, Pallas kernels, layer(): pl.pallas_call(functools.partial(layer_kernel, n_sp, n_tp, inner, el, cap...  90 us

profile of v2, /device:TPU:0, one launch (start us, length us, event | category | flops | bytes accessed | tf_op | source)
XLA Modules:
  0.0 91.7 jit_solution(7291918220577087980)
XLA Ops:
  0.0 90.0 %shard_map.145 = bf16[128,1024]{1,0:T(8,128)(2,1)} custom-call(bf16[128,512]{1,0:T(8,128)(2,1)} %refs_0_.1, bf16[128,512]{1,0:T(8,128)(2,1)} %refs_1_.1, bf16[128,512]{1,0:T(8,128)(2,1)} %refs_2_.1, bf16[4,128]{1,0:T(4,128)(2,1)} %bitcast.5, bf16[128,1024]{1,0:T(8,128)(2,1)} %refs_4_.1, bf16[2048,1024]{1,0:T(8,128)(2,1)} %refs_5_.1, f32[1,1024]{1,0:T(1,128)} %bitcast.4, ...), custom_call_target="tpu_custom_call" | custom-call | flops 10000000000 | bytes 16777216 | tf_op jit(solution)/shard_map/pallas_call | solution.py:1060
  90.0 1.7 %copy.17 = bf16[128,1024]{1,0:T(8,128)(2,1)} copy(bf16[128,1024]{1,0:T(8,128)(2,1)} %shard_map.145) | data formatting | bytes 524288

commit v3 on v2

--- a/solution.py
+++ b/solution.py
@@ -294,18 +294,8 @@
 
 
 def plane_order(z, outer):
-    if outer != 4:
-        return [(z + i) % outer for i in range(outer)]
-    middle = ((z + 1) // 2) % 2
-    near = z + 1 - 2 * (z % 2)
-    across = 3 - z
-    two = (z + 2) % 4
-    return [
-        z,
-        near,
-        middle * across + (1 - middle) * two,
-        middle * two + (1 - middle) * across,
-    ]
+    step = 1 - 2 * ((2 * z) // outer)
+    return [(z + step * i + outer) % outer for i in range(outer)]
 
 
 def greet_all(n_sp, n_tp, own, me):
@@ -318,7 +308,10 @@
         pl.semaphore_signal(
             barrier, inc=1, device_id={"tp": (me + d) % n_tp}, device_id_type=MESH
         )
-    pl.semaphore_wait(barrier, n_sp + n_tp - 2)
+
+
+def await_all(n_sp, n_tp):
+    pl.semaphore_wait(pltpu.get_barrier_semaphore(), n_sp + n_tp - 2)
 
 
 class Experts:
@@ -333,6 +326,12 @@
         self.z = self.own // inner
         self.x = self.own % inner
         self.order = plane_order(self.z, self.outer)
+        self.side = self.z // 2
+        self.within = self.z % 2
+        self.mate = self.z + 1 - 2 * self.within
+        self.middle = 1 + self.side
+        self.between = (self.z > 0) & (self.z < self.outer - 1)
+        self.at_end = jnp.logical_not(self.between)
         self.tok, self.width = self.mixed.shape
         self.ff = self.down.shape[1]
         self.total_width = self.width * n_tp
@@ -389,7 +388,10 @@
             mine = jnp.sum(jnp.where(named[k], rank, 0.0), axis=0, keepdims=True)
             slot = ids[k : k + 1, :].astype(F32) * self.cap + mine
             self.meta[self.own, k : k + 1, :] = slot
+            self.meta[self.own, top_k + k : top_k + k + 1, :] = self.wts[k : k + 1, :]
         self.top_k = top_k
+
+    def send_route(self):
         self.meta_group = self.meta_copies(self.meta, self.meta_s, self.meta_r)
         for c in self.meta_group:
             c.start()
@@ -400,14 +402,20 @@
         ).astype(F32)
         return [self.meta[block, k : k + 1, :] == spot for k in range(self.top_k)]
 
+    def back_of(self, block, plane):
+        rows = self.inner * self.rw
+        hits = self.slot_hits(block, plane * rows, rows)
+        weight = sum(
+            jnp.where(
+                hits[k], self.meta[block, self.top_k + k : self.top_k + k + 1, :], 0.0
+            )
+            for k in range(self.top_k)
+        )
+        return jnp.transpose(weight).astype(BF16)
+
     def build_back(self):
-        rows = self.inner * self.rw
-        for plane in range(self.outer):
-            hits = self.slot_hits(self.own, plane * rows, rows)
-            weight = sum(
-                jnp.where(hits[k], self.wts[k : k + 1, :], 0.0) for k in range(self.top_k)
-            )
-            self.back[plane] = jnp.transpose(weight).astype(BF16)
+        self.back[0] = self.back_of(self.own, self.z)
+        self.back[1] = self.back_of(self.own, self.mate)
 
     def dense_copy(self, src, plane, step):
         return rcopy(
@@ -434,8 +442,7 @@
         def _():
             act(self.dense_copy(self.dense.at[plane], plane, -1))
 
-    def take_dense(self, i):
-        plane = self.order[i]
+    def receive(self, plane):
         rcopy(
             self.dense.at[plane],
             self.dense.at[plane],
@@ -444,6 +451,22 @@
             {"sp": (self.own + 1) % self.n_sp},
         ).wait_recv()
         self.hand_on(plane, lambda c: c.start())
+
+    def take_dense(self, i):
+        last = self.outer - 1
+        if i == last:
+
+            @pl.when(self.at_end)
+            def _():
+                self.receive(self.order[i])
+
+            return
+        self.receive(self.order[i])
+        if i == 1:
+
+            @pl.when(self.between)
+            def _():
+                self.receive(self.order[last])
 
     def cross_copies(self, i):
         return [
@@ -594,6 +617,78 @@
             for d in range(0 if i else 1, self.inner)
         ]
 
+    def halves(self):
+        half = self.width // 2
+        return [pl.ds(h * half, half) for h in range(2)]
+
+    def over_copies(self, i, c, first):
+        return [
+            rcopy(
+                self.outs.at[i, (self.x + d) % self.inner, :, cols],
+                self.over.at[c, self.within, self.x, :, cols],
+                self.over_s.at[i, d, h],
+                self.over_r.at[c, self.within, self.x, h],
+                {"sp": self.middle * self.inner + (self.x + d) % self.inner},
+            )
+            for h, cols in enumerate(self.halves())
+            for d in range(first, self.inner)
+        ]
+
+    def each_return(self, i, act):
+        if i == 0:
+            act(self.return_copies(0))
+            return
+
+        @pl.when(self.at_end)
+        def _():
+            act(self.over_copies(i, i - 2, 0) if i > 1 else self.return_copies(i))
+
+        @pl.when(self.between)
+        def _():
+            act(self.over_copies(i, i - 1, 1) if i < 3 else self.return_copies(i))
+
+    def sum_copy(self, c, h):
+        cols = self.halves()[h]
+        return rcopy(
+            self.sums.at[c, :, cols],
+            self.far.at[:, cols],
+            self.sum_s.at[c, h],
+            self.far_r.at[h],
+            {"sp": self.order[c + 1] * self.inner + self.x},
+        )
+
+    def add_over(self, c):
+        block = self.order[c + 1] * self.inner + self.x
+        pair = 2 * self.side
+        backs = [self.back_of(block, pair + s) for s in range(2)]
+        for h, cols in enumerate(self.halves()):
+
+            def arrived(s, x_from):
+                piece = self.over.at[c, s, x_from, :, cols]
+                rcopy(
+                    piece,
+                    piece,
+                    self.over_s.at[0, 0, h],
+                    self.over_r.at[c, s, x_from, h],
+                    {"sp": (self.own + 1) % self.n_sp},
+                ).wait_recv()
+
+            total = 0.0
+            for s in range(2):
+                for d in range(1, self.inner):
+                    arrived(s, (self.x + d) % self.inner)
+
+                @pl.when(self.within != s)
+                def _():
+                    arrived(s, self.x)
+
+                rows = jnp.concatenate(
+                    [self.over[c, s, p, :, cols] for p in range(self.inner)], axis=0
+                )
+                total = total + jnp.dot(backs[s], rows, preferred_element_type=F32)
+            self.sums[c, :, cols] = total.astype(BF16)
+            self.sum_copy(c, h).start()
+
     def down_rows(self, i):
         if i == 0:
             self.loads[4].wait()
@@ -607,10 +702,19 @@
                 self.outs[i, p, e * self.cap : (e + 1) * self.cap, :] = out[
                     p * self.cap : (p + 1) * self.cap
                 ]
-        for c in self.return_copies(i):
-            c.start()
+
+        def start(group):
+            for c in group:
+                c.start()
+
+        self.each_return(i, start)
         if i == 0:
             self.ret[self.own] = self.outs[0, self.x]
+        elif i < 3:
+
+            @pl.when(self.between)
+            def _():
+                self.over[i - 1, self.within, self.x] = self.outs[i, self.x]
 
     def shared_down(self):
         self.loads[5].wait()
@@ -619,25 +723,29 @@
         )
         self.acc[...] = self.mixed[...].astype(F32) + shared
 
-    def collect(self, i, last=False):
-        plane = self.order[i]
-        for d in range(0 if i else 1, self.inner):
+    def collect(self, n):
+        plane = (self.z, self.mate)[n]
+        for d in range(1 - n, self.inner):
             block = plane * self.inner + (self.x + d) % self.inner
             rcopy(
                 self.ret.at[block],
                 self.ret.at[block],
-                self.ret_s.at[i, d],
+                self.ret_s.at[n, d],
                 self.ret_r.at[block],
                 {"sp": (self.own + 1) % self.n_sp},
             ).wait_recv()
         rows = jnp.concatenate(
             [self.ret[plane * self.inner + p] for p in range(self.inner)], axis=0
         )
-        got = jnp.dot(self.back[plane], rows, preferred_element_type=F32)
-        if last:
-            self.out[...] = (self.acc[...] + got).astype(BF16)
-        else:
-            self.acc[...] += got
+        self.acc[...] += jnp.dot(self.back[n], rows, preferred_element_type=F32)
+
+    def close(self):
+        for h, cols in enumerate(self.halves()):
+            piece = self.far.at[:, cols]
+            rcopy(
+                piece, piece, self.sum_s.at[0, h], self.far_r.at[h], {"sp": (self.own + 1) % self.n_sp}
+            ).wait_recv()
+            self.out[:, cols] = (self.acc[:, cols] + self.far[:, cols].astype(F32)).astype(BF16)
 
     def finish(self):
         def sent(c):
@@ -649,10 +757,22 @@
         groups = [self.meta_group, self.inv_group, self.ssq_group]
         groups += list(self.part_groups.values()) + list(self.hid_groups.values())
         groups += [self.cross_copies(i) for i in range(self.outer)]
-        groups += [self.return_copies(i) for i in range(self.outer)]
         for group in groups:
             for c in group:
                 c.wait_send()
+
+        def all_sent(group):
+            for c in group:
+                c.wait_send()
+
+        for i in range(self.outer):
+            self.each_return(i, all_sent)
+
+        @pl.when(self.between)
+        def _():
+            for c in range(2):
+                for h in range(2):
+                    self.sum_copy(c, h).wait_send()
 
     def run(self):
         outer = self.outer
@@ -663,20 +783,29 @@
         self.send_scales()
         self.shared_gate_up()
         self.gate_up(0)
-        for i in range(1, outer + 1):
+        for i in range(1, outer + 2):
             if i < outer:
                 self.take_dense(i)
                 self.select(i)
+            if i > 1:
+                self.down_rows(i - 2)
             if i == 1:
                 self.hidden(outer)
-            self.hidden(i - 1)
+            if i <= outer:
+                self.hidden(i - 1)
             if i == 1:
                 self.shared_down()
             if i < outer:
                 self.gate_up(i)
-            self.down_rows(i - 1)
-        for i in range(outer):
-            self.collect(i, i == outer - 1)
+        self.collect(0)
+
+        @pl.when(self.between)
+        def _():
+            for c in range(2):
+                self.add_over(c)
+
+        self.collect(1)
+        self.close()
         self.finish()
 
 
@@ -702,7 +831,10 @@
         "hid": vmem((outer + 1, n_tp, chunk, ff), BF16),
         "outs": vmem((outer, inner, rw, width), BF16),
         "ret": vmem((n_sp, rw, width), BF16),
-        "back": vmem((outer, tok, inner * rw), BF16),
+        "back": vmem((2, tok, inner * rw), BF16),
+        "over": vmem((2, 2, inner, rw, width), BF16),
+        "sums": vmem((2, tok, width), BF16),
+        "far": vmem((tok, width), BF16),
         "acc": vmem((tok, width), F32),
         "w_sem": dma((6,)),
         "meta_s": dma((n_sp,)),
@@ -721,6 +853,10 @@
         "hid_r": dma((outer + 1, n_tp)),
         "ret_s": dma((outer, inner)),
         "ret_r": dma((n_sp,)),
+        "over_s": dma((outer, inner, 2)),
+        "over_r": dma((2, 2, inner, 2)),
+        "sum_s": dma((2, 2)),
+        "far_r": dma((2,)),
     }
 
 
@@ -1035,13 +1171,15 @@
     for c in small:
         c.start()
     greet_all(n_sp, n_tp, first.own, first.me)
-    first.exchange()
     first.load_late()
     second.load_weights()
     for c in small:
         c.wait()
     second.route()
     second.build_back()
+    await_all(n_sp, n_tp)
+    first.exchange()
+    second.send_route()
     first.hand_over()
     first.compute()
     first.gather()
@@ -1102,7 +1240,7 @@
     cap = 2 * top_k * tok // experts
     n_inner = max(d for d in range(1, n_sp + 1) if n_sp % d == 0 and d * d <= n_sp)
     plane_rows = n_inner * experts_local * cap
-    if heads * n_inner == n_sp and plane_rows == tok and cap % 16 == 0 and tok % (16 * n_tp) == 0:
+    if heads * n_inner == n_sp and heads == 4 and plane_rows == tok and cap % 16 == 0 and tok % (16 * n_tp) == 0:
         operands = (
             queries, key_rows, value_rows, break_bias.T, stream, out_proj, norm_gain[None, :],
             expert_ids.T, route_weights.T, gate_proj, up_proj, down_proj,

time: 91.8 us -> 85 us (0.926)
  Pallas kernels: 90 us -> 83.2 us
    pallas_call x1, Pallas kernels: 90 us -> 83.2 us  [layer(): pl.pallas_call(functools.partial(layer_kernel, n_sp, n_tp, inner, el, cap...]
where the time goes in v3:
time: 85 us; the launch traced here: 84.8 us
  Pallas kernels  83.2 us (98%)
  local copies, waits for them, and re-layouts  1.67 us (2%)
    pallas_call x1, Pallas kernels, layer(): pl.pallas_call(functools.partial(layer_kernel, n_sp, n_tp, inner, el, cap...  83.2 us

profile of v3, /device:TPU:0, one launch (start us, length us, event | category | flops | bytes accessed | tf_op | source)
XLA Modules:
  0.0 84.8 jit_solution(13287823013890250667)
XLA Ops:
  0.0 83.2 %shard_map.145 = bf16[128,1024]{1,0:T(8,128)(2,1)} custom-call(bf16[128,512]{1,0:T(8,128)(2,1)} %refs_0_.1, bf16[128,512]{1,0:T(8,128)(2,1)} %refs_1_.1, bf16[128,512]{1,0:T(8,128)(2,1)} %refs_2_.1, bf16[4,128]{1,0:T(4,128)(2,1)} %bitcast.5, bf16[128,1024]{1,0:T(8,128)(2,1)} %refs_4_.1, bf16[2048,1024]{1,0:T(8,128)(2,1)} %refs_5_.1, f32[1,1024]{1,0:T(1,128)} %bitcast.4, ...), custom_call_target="tpu_custom_call" | custom-call | flops 10000000000 | bytes 16777216 | tf_op jit(solution)/shard_map/pallas_call | solution.py:1198
  83.2 1.7 %copy.17 = bf16[128,1024]{1,0:T(8,128)(2,1)} copy(bf16[128,1024]{1,0:T(8,128)(2,1)} %shard_map.145) | data formatting | bytes 524288

commit v4 on v3

--- a/solution.py
+++ b/solution.py
@@ -276,6 +276,7 @@
 
 
 MESH = pl.DeviceIdType.MESH
+CUTS = 4
 
 
 def rows_contract(lhs, rhs):
@@ -325,11 +326,14 @@
         self.me = lax.axis_index("tp")
         self.z = self.own // inner
         self.x = self.own % inner
-        self.order = plane_order(self.z, self.outer)
         self.side = self.z // 2
         self.within = self.z % 2
         self.mate = self.z + 1 - 2 * self.within
         self.middle = 1 + self.side
+        self.order = [self.z, 2 - self.side, 3 - 3 * self.side, self.mate]
+        self.core = self.me % 2
+        self.partner = self.me + 1 - 2 * self.core
+        self.chip = self.me // 2
         self.between = (self.z > 0) & (self.z < self.outer - 1)
         self.at_end = jnp.logical_not(self.between)
         self.tok, self.width = self.mixed.shape
@@ -396,6 +400,10 @@
         for c in self.meta_group:
             c.start()
 
+    def wait_route(self):
+        for d in range(1, self.n_sp):
+            self.wait_table(self.meta, self.meta_s, self.meta_r, (self.own + d) % self.n_sp)
+
     def slot_hits(self, block, first, count):
         spot = (
             lax.broadcasted_iota(jnp.int32, (count, self.tok), 0) + first
@@ -417,76 +425,80 @@
         self.back[0] = self.back_of(self.own, self.z)
         self.back[1] = self.back_of(self.own, self.mate)
 
-    def dense_copy(self, src, plane, step):
-        return rcopy(
-            src,
-            self.dense.at[plane],
-            self.dense_s.at[plane, (step + 1) // 2],
-            self.dense_r.at[plane],
-            {"sp": (self.z + step) * self.inner + self.x},
-        )
-
-    def spread_own(self, act):
-        for step in (1, -1):
-
-            @pl.when(self.z < self.outer - 1 if step == 1 else self.z > 0)
-            def _():
-                act(self.dense_copy(self.mixed, self.z, step))
-
-    def hand_on(self, plane, act):
-        @pl.when((plane < self.z) & (self.z < self.outer - 1))
-        def _():
-            act(self.dense_copy(self.dense.at[plane], plane, 1))
-
-        @pl.when((plane > self.z) & (self.z > 0))
-        def _():
-            act(self.dense_copy(self.dense.at[plane], plane, -1))
-
-    def receive(self, plane):
+    def halves(self):
+        half = self.width // 2
+        return [pl.ds(h * half, half) for h in range(2)]
+
+    def dense_copies(self, src, plane, target, only=None):
+        return [
+            rcopy(
+                src.at[:, cols],
+                self.dense.at[plane, :, cols],
+                self.dense_s.at[plane, h],
+                self.dense_r.at[plane, h],
+                {"sp": target * self.inner + self.x},
+            )
+            for h, cols in enumerate(self.halves())
+            if only is None or h == only
+        ]
+
+    def own_copies(self):
+        at_end = self.at_end.astype(jnp.int32)
+        target = at_end * self.mate + (1 - at_end) * (3 - self.z)
+        return self.dense_copies(self.mixed, self.z, target)
+
+    def relay_copies(self, only=None):
+        return self.dense_copies(self.dense.at[self.mate], self.mate, 3 - self.z, only)
+
+    def receive(self, plane, h):
+        piece = self.dense.at[plane, :, self.halves()[h]]
         rcopy(
-            self.dense.at[plane],
-            self.dense.at[plane],
-            self.dense_s.at[plane, 0],
-            self.dense_r.at[plane],
-            {"sp": (self.own + 1) % self.n_sp},
+            piece, piece, self.dense_s.at[plane, h], self.dense_r.at[plane, h], {"sp": (self.own + 1) % self.n_sp}
         ).wait_recv()
-        self.hand_on(plane, lambda c: c.start())
-
-    def take_dense(self, i):
-        last = self.outer - 1
-        if i == last:
-
-            @pl.when(self.at_end)
-            def _():
-                self.receive(self.order[i])
-
-            return
-        self.receive(self.order[i])
-        if i == 1:
-
-            @pl.when(self.between)
-            def _():
-                self.receive(self.order[last])
+
+    def pick_rows(self, block, plane):
+        rows = self.inner * self.rw
+        hits = self.slot_hits(block, plane * rows, rows)
+        return functools.reduce(jnp.logical_or, hits).astype(F32).astype(BF16)
+
+    def ahead_copies(self, i, h):
+        cols = self.halves()[h]
+        return [
+            rcopy(
+                self.ahead.at[i, (self.x + d) % self.inner, :, cols],
+                self.rows.at[i or 3, self.x, :, cols],
+                self.ahead_s.at[i, d, h],
+                self.x_r.at[i or 3, self.x, h],
+                {"sp": self.mate * self.inner + (self.x + d) % self.inner},
+            )
+            for d in range(self.inner)
+        ]
+
+    def push(self, i, h):
+        cols = self.halves()[h]
+        pick = self.pick_rows(self.order[i] * self.inner + self.x, self.mate)
+        source = self.dense[self.order[i], :, cols] if i else self.mixed[:, cols]
+        got = jnp.dot(pick, source, preferred_element_type=F32).astype(BF16)
+        for p in range(self.inner):
+            self.ahead[i, p, :, cols] = got[p * self.rw : (p + 1) * self.rw]
+        for c in self.ahead_copies(i, h):
+            c.start()
 
     def cross_copies(self, i):
         return [
             rcopy(
-                self.picked.at[i, (self.x + d) % self.inner],
-                self.rows.at[i, self.x],
-                self.x_s.at[i, d],
-                self.x_r.at[i, self.x],
+                self.picked.at[i, (self.x + d) % self.inner, :, cols],
+                self.rows.at[i, self.x, :, cols],
+                self.x_s.at[i, d, h],
+                self.x_r.at[i, self.x, h],
                 {"sp": self.z * self.inner + (self.x + d) % self.inner},
             )
+            for h, cols in enumerate(self.halves())
             for d in range(1, self.inner)
         ]
 
     def select(self, i):
-        block = self.order[i] * self.inner + self.x
-        if i:
-            self.wait_table(self.meta, self.meta_s, self.meta_r, block)
-        rows = self.inner * self.rw
-        hits = self.slot_hits(block, self.z * rows, rows)
-        pick = functools.reduce(jnp.logical_or, hits).astype(F32).astype(BF16)
+        pick = self.pick_rows(self.order[i] * self.inner + self.x, self.z)
         source = self.dense[self.order[i]] if i else self.mixed[...]
         got = jnp.dot(pick, source, preferred_element_type=F32).astype(BF16)
         for p in range(self.inner):
@@ -494,6 +506,27 @@
         for c in self.cross_copies(i):
             c.start()
         self.rows[i, self.x] = self.picked[i, self.x]
+
+    def wait_rows(self, i):
+        def arrived(x_from):
+            for h, cols in enumerate(self.halves()):
+                piece = self.rows.at[i, x_from, :, cols]
+                rcopy(
+                    piece,
+                    piece,
+                    self.x_s.at[i, 0, h],
+                    self.x_r.at[i, x_from, h],
+                    {"sp": (self.own + 1) % self.n_sp},
+                ).wait_recv()
+
+        if i:
+
+            @pl.when(self.at_end)
+            def _():
+                arrived(self.x)
+
+        for d in range(1, self.inner):
+            arrived((self.x + d) % self.inner)
 
     def tp_copies(self, src, dst, send, recv):
         return [
@@ -529,35 +562,55 @@
         for c in self.inv_group:
             c.start()
 
+    def part_copy(self, s):
+        return rcopy(
+            self.gu.at[s, 1 - self.core],
+            self.parts.at[s],
+            self.part_s.at[s],
+            self.part_r.at[s],
+            {"tp": self.partner},
+        )
+
+    def pair_copies(self, s):
+        return [
+            rcopy(
+                self.pairs.at[s],
+                self.sides.at[s, self.chip],
+                self.pair_s.at[s, d],
+                self.pair_r.at[s, self.chip],
+                {"tp": (self.me + 2 * d) % self.n_tp},
+            )
+            for d in range(1, self.n_tp // 2)
+        ]
+
+    def hid_copy(self, s):
+        mine = self.hid.at[s, self.core]
+        return rcopy(
+            mine, mine, self.hid_s.at[s], self.hid_r.at[s], {"tp": self.partner}
+        )
+
     def send_parts(self, s, value):
-        chunk = value.shape[0] // self.n_tp
-        for p in range(self.n_tp):
-            self.gu[s, p] = value[p * chunk : (p + 1) * chunk]
-        group = self.tp_copies(
-            lambda to: self.gu.at[s, to], self.parts.at[s, self.me], self.part_s.at[s], self.part_r.at[s]
-        )
-        for c in group:
+        half = value.shape[0] // 2
+        for c in range(2):
+            self.gu[s, c] = value[c * half : (c + 1) * half]
+        self.part_copy(s).start()
+
+    def pair(self, s):
+        self.part_copy(s).wait_recv()
+        self.pairs[s] = (
+            self.gu[s, self.core].astype(F32) + self.parts[s].astype(F32)
+        ).astype(BF16)
+        for c in self.pair_copies(s):
             c.start()
-        self.part_groups[s] = group
 
     def gate_up(self, i):
         if i == 0:
             self.loads[2].wait()
             self.loads[3].wait()
-        for d in range(1, self.inner):
-            x_from = (self.x + d) % self.inner
-            rcopy(
-                self.rows.at[i, x_from],
-                self.rows.at[i, x_from],
-                self.x_s.at[i, d],
-                self.x_r.at[i, x_from],
-                {"sp": (self.own + 1) % self.n_sp},
-            ).wait_recv()
+        self.wait_rows(i)
         normed = []
         for d in range(self.inner):
             block = self.order[i] * self.inner + (self.x + d) % self.inner
-            if d:
-                self.wait_table(self.meta, self.meta_s, self.meta_r, block)
             if i or d:
                 self.wait_table(self.inv, self.inv_s, self.inv_r, block)
         for p in range(self.inner):
@@ -588,22 +641,29 @@
         self.send_parts(self.outer, value)
 
     def hidden(self, s):
-        self.tp_wait(lambda other: self.parts.at[s, other], self.part_s.at[s], self.part_r.at[s])
-        total = self.gu[s, self.me].astype(F32)
-        for d in range(1, self.n_tp):
-            total = total + self.parts[s, (self.me + d) % self.n_tp].astype(F32)
+        total = self.pairs[s].astype(F32)
+        for d in range(1, self.n_tp // 2):
+            other = (self.chip + d) % (self.n_tp // 2)
+            rcopy(
+                self.sides.at[s, other],
+                self.sides.at[s, other],
+                self.pair_s.at[s, d],
+                self.pair_r.at[s, other],
+                {"tp": self.partner},
+            ).wait_recv()
+            total = total + self.sides[s, other].astype(F32)
         act = jax.nn.silu(total[:, : self.ff]) * total[:, self.ff :]
-        self.hid[s, self.me] = act.astype(BF16)
-        group = self.tp_copies(
-            lambda to: self.hid.at[s, self.me], self.hid.at[s, self.me], self.hid_s.at[s], self.hid_r.at[s]
-        )
-        for c in group:
-            c.start()
-        self.hid_groups[s] = group
+        self.hid[s, self.core] = act.astype(BF16)
+        self.hid_copy(s).start()
 
     def all_hidden(self, s):
-        self.tp_wait(lambda other: self.hid.at[s, other], self.hid_s.at[s], self.hid_r.at[s])
-        return jnp.concatenate([self.hid[s, p] for p in range(self.n_tp)], axis=0)
+        other = self.hid.at[s, 1 - self.core]
+        rcopy(other, other, self.hid_s.at[s], self.hid_r.at[s], {"tp": self.partner}).wait_recv()
+        return jnp.concatenate([self.hid[s, c] for c in range(2)], axis=0)
+
+    def cuts(self):
+        cut = self.width // CUTS
+        return [pl.ds(h * cut, cut) for h in range(CUTS)]
 
     def return_copies(self, i):
         return [
@@ -617,10 +677,6 @@
             for d in range(0 if i else 1, self.inner)
         ]
 
-    def halves(self):
-        half = self.width // 2
-        return [pl.ds(h * half, half) for h in range(2)]
-
     def over_copies(self, i, c, first):
         return [
             rcopy(
@@ -630,25 +686,70 @@
                 self.over_r.at[c, self.within, self.x, h],
                 {"sp": self.middle * self.inner + (self.x + d) % self.inner},
             )
-            for h, cols in enumerate(self.halves())
+            for h, cols in enumerate(self.cuts())
             for d in range(first, self.inner)
         ]
 
-    def each_return(self, i, act):
+    def side_out_copies(self, i):
+        return [
+            rcopy(
+                self.outs.at[i, (self.x + d) % self.inner, :, cols],
+                self.beside.at[i - 1, self.x, :, cols],
+                self.beside_s.at[i - 1, d, h],
+                self.beside_r.at[i - 1, self.x, h],
+                {"sp": self.z * self.inner + (self.x + d) % self.inner},
+            )
+            for h, cols in enumerate(self.cuts())
+            for d in range(1, self.inner)
+        ]
+
+    def column_copies(self, i, d, h):
+        cols = self.cuts()[h]
+        x_of = (self.x + d) % self.inner
+        src = self.beside.at[i - 1, x_of, :, cols] if d else self.outs.at[i, self.x, :, cols]
+        if i == 3:
+            dst = self.ret.at[self.z * self.inner + x_of, :, cols]
+            arrived = self.ret_h.at[x_of, h]
+        else:
+            dst = self.over.at[i - 1, self.within, x_of, :, cols]
+            arrived = self.over_r.at[i - 1, self.within, x_of, h]
+        return [
+            rcopy(src, dst, self.over_s.at[i, d, h], arrived, {"sp": self.mate * self.inner + self.x})
+        ]
+
+    def bring_along(self, i):
+        for h, cols in enumerate(self.cuts()):
+            for d in range(1, self.inner):
+                x_of = (self.x + d) % self.inner
+                piece = self.beside.at[i - 1, x_of, :, cols]
+                rcopy(
+                    piece,
+                    piece,
+                    self.beside_s.at[i - 1, d, h],
+                    self.beside_r.at[i - 1, x_of, h],
+                    {"sp": (self.own + 1) % self.n_sp},
+                ).wait_recv()
+                for c in self.column_copies(i, d, h):
+                    c.start()
+
+    def each_return(self, i, act, sent=False):
         if i == 0:
             act(self.return_copies(0))
             return
 
         @pl.when(self.at_end)
         def _():
-            act(self.over_copies(i, i - 2, 0) if i > 1 else self.return_copies(i))
+            act(self.side_out_copies(i))
+            for h in range(CUTS):
+                for d in range(self.inner if sent else 1):
+                    act(self.column_copies(i, d, h))
 
         @pl.when(self.between)
         def _():
             act(self.over_copies(i, i - 1, 1) if i < 3 else self.return_copies(i))
 
     def sum_copy(self, c, h):
-        cols = self.halves()[h]
+        cols = self.cuts()[h]
         return rcopy(
             self.sums.at[c, :, cols],
             self.far.at[:, cols],
@@ -661,7 +762,7 @@
         block = self.order[c + 1] * self.inner + self.x
         pair = 2 * self.side
         backs = [self.back_of(block, pair + s) for s in range(2)]
-        for h, cols in enumerate(self.halves()):
+        for h, cols in enumerate(self.cuts()):
 
             def arrived(s, x_from):
                 piece = self.over.at[c, s, x_from, :, cols]
@@ -725,7 +826,8 @@
 
     def collect(self, n):
         plane = (self.z, self.mate)[n]
-        for d in range(1 - n, self.inner):
+
+        def whole(d):
             block = plane * self.inner + (self.x + d) % self.inner
             rcopy(
                 self.ret.at[block],
@@ -734,13 +836,37 @@
                 self.ret_r.at[block],
                 {"sp": (self.own + 1) % self.n_sp},
             ).wait_recv()
+
+        def in_halves(d):
+            x_of = (self.x + d) % self.inner
+            for h, cols in enumerate(self.cuts()):
+                piece = self.ret.at[plane * self.inner + x_of, :, cols]
+                rcopy(
+                    piece, piece, self.ret_s.at[n, d], self.ret_h.at[x_of, h], {"sp": (self.own + 1) % self.n_sp}
+                ).wait_recv()
+
+        if n == 0:
+            for d in range(1, self.inner):
+                whole(d)
+        else:
+
+            @pl.when(self.at_end)
+            def _():
+                for d in range(self.inner):
+                    whole(d)
+
+            @pl.when(self.between)
+            def _():
+                for d in range(self.inner):
+                    in_halves(d)
+
         rows = jnp.concatenate(
             [self.ret[plane * self.inner + p] for p in range(self.inner)], axis=0
         )
         self.acc[...] += jnp.dot(self.back[n], rows, preferred_element_type=F32)
 
     def close(self):
-        for h, cols in enumerate(self.halves()):
+        for h, cols in enumerate(self.cuts()):
             piece = self.far.at[:, cols]
             rcopy(
                 piece, piece, self.sum_s.at[0, h], self.far_r.at[h], {"sp": (self.own + 1) % self.n_sp}
@@ -748,15 +874,10 @@
             self.out[:, cols] = (self.acc[:, cols] + self.far[:, cols].astype(F32)).astype(BF16)
 
     def finish(self):
-        def sent(c):
-            c.wait_send()
-
-        self.spread_own(sent)
-        for i in range(1, self.outer):
-            self.hand_on(self.order[i], sent)
         groups = [self.meta_group, self.inv_group, self.ssq_group]
-        groups += list(self.part_groups.values()) + list(self.hid_groups.values())
-        groups += [self.cross_copies(i) for i in range(self.outer)]
+        for n in range(self.outer + 1):
+            groups += [[self.part_copy(n)], self.pair_copies(n), [self.hid_copy(n)]]
+        groups += [self.cross_copies(0), self.own_copies()]
         for group in groups:
             for c in group:
                 c.wait_send()
@@ -766,44 +887,85 @@
                 c.wait_send()
 
         for i in range(self.outer):
-            self.each_return(i, all_sent)
+            self.each_return(i, all_sent, True)
 
         @pl.when(self.between)
         def _():
+            all_sent(self.relay_copies())
+            for i in range(1, self.outer):
+                all_sent(self.cross_copies(i))
+            for h in range(2):
+                for i in range(self.outer - 1):
+                    all_sent(self.ahead_copies(i, h))
             for c in range(2):
-                for h in range(2):
+                for h in range(CUTS):
                     self.sum_copy(c, h).wait_send()
 
+    def middle_only(self, *steps):
+        @pl.when(self.between)
+        def _():
+            for step in steps:
+                step()
+
+    def end_only(self, step):
+        @pl.when(self.at_end)
+        def _():
+            step()
+
+    def relay(self, h):
+        self.receive(self.mate, h)
+        for c in self.relay_copies(h):
+            c.start()
+
+    def pass_on(self, i, h):
+        self.receive(self.order[i], h)
+        self.push(i, h)
+
     def run(self):
-        outer = self.outer
-        self.part_groups, self.hid_groups = {}, {}
-        self.spread_own(lambda c: c.start())
+        for c in self.own_copies():
+            c.start()
+        self.wait_route()
+        self.middle_only(lambda: self.push(0, 0))
         self.send_squares()
         self.select(0)
+        self.middle_only(lambda: self.relay(0), lambda: self.pass_on(1, 0))
         self.send_scales()
+        self.middle_only(
+            lambda: self.relay(1), lambda: self.pass_on(1, 1), lambda: self.select(1)
+        )
+        shared = self.outer
         self.shared_gate_up()
         self.gate_up(0)
-        for i in range(1, outer + 2):
-            if i < outer:
-                self.take_dense(i)
-                self.select(i)
-            if i > 1:
-                self.down_rows(i - 2)
-            if i == 1:
-                self.hidden(outer)
-            if i <= outer:
-                self.hidden(i - 1)
-            if i == 1:
-                self.shared_down()
-            if i < outer:
-                self.gate_up(i)
+        self.pair(shared)
+        self.pair(0)
+        self.middle_only(
+            lambda: self.pass_on(2, 0),
+            lambda: self.pass_on(2, 1),
+            lambda: self.push(0, 1),
+            lambda: self.select(2),
+            lambda: self.select(3),
+        )
+        self.gate_up(1)
+        self.hidden(shared)
+        self.hidden(0)
+        self.pair(1)
+        self.shared_down()
+        self.down_rows(0)
+        self.gate_up(2)
+        self.hidden(1)
+        self.pair(2)
+        self.gate_up(3)
+        self.down_rows(1)
+        self.pair(3)
+        self.hidden(2)
+        self.end_only(lambda: self.bring_along(1))
+        self.down_rows(2)
+        self.hidden(3)
+        self.end_only(lambda: self.bring_along(2))
+        self.down_rows(3)
         self.collect(0)
-
-        @pl.when(self.between)
-        def _():
-            for c in range(2):
-                self.add_over(c)
-
+        self.end_only(lambda: self.bring_along(3))
+        self.middle_only(lambda: self.add_over(0), lambda: self.add_over(1))
         self.collect(1)
         self.close()
         self.finish()
@@ -811,9 +973,7 @@
 
 def moe_scratch(n_sp, n_tp, inner, el, cap, tok, width, ff):
     outer, rw = n_sp // inner, el * cap
-    chunk = inner * rw // n_tp
-    chunk_s = tok // n_tp
-    assert chunk == chunk_s
+    assert inner * rw == tok
     vmem, dma = pltpu.VMEM, pltpu.SemaphoreType.DMA
     return {
         "wgu": vmem((el, width, 2 * ff), BF16),
@@ -821,14 +981,17 @@
         "wsgu": vmem((width, 2 * ff), BF16),
         "wsd": vmem((ff, width), BF16),
         "dense": vmem((outer, tok, width), BF16),
+        "ahead": vmem((outer - 1, inner, rw, width), BF16),
         "picked": vmem((outer, inner, rw, width), BF16),
         "rows": vmem((outer, inner, rw, width), BF16),
         "meta": vmem((n_sp, 8, tok), F32),
         "inv": vmem((n_sp, 8, tok), F32),
         "ssq": vmem((n_tp, 8, tok), F32),
-        "gu": vmem((outer + 1, n_tp, chunk, 2 * ff), BF16),
-        "parts": vmem((outer + 1, n_tp, chunk, 2 * ff), BF16),
-        "hid": vmem((outer + 1, n_tp, chunk, ff), BF16),
+        "gu": vmem((outer + 1, 2, tok // 2, 2 * ff), BF16),
+        "parts": vmem((outer + 1, tok // 2, 2 * ff), BF16),
+        "pairs": vmem((outer + 1, tok // 2, 2 * ff), BF16),
+        "sides": vmem((outer + 1, n_tp // 2, tok // 2, 2 * ff), BF16),
+        "hid": vmem((outer + 1, 2, tok // 2, ff), BF16),
         "outs": vmem((outer, inner, rw, width), BF16),
         "ret": vmem((n_sp, rw, width), BF16),
         "back": vmem((2, tok, inner * rw), BF16),
@@ -844,19 +1007,26 @@
         "ssq_s": dma((n_tp,)),
         "ssq_r": dma((n_tp,)),
         "dense_s": dma((outer, 2)),
-        "dense_r": dma((outer,)),
-        "x_s": dma((outer, inner)),
-        "x_r": dma((outer, inner)),
-        "part_s": dma((outer + 1, n_tp)),
-        "part_r": dma((outer + 1, n_tp)),
-        "hid_s": dma((outer + 1, n_tp)),
-        "hid_r": dma((outer + 1, n_tp)),
+        "dense_r": dma((outer, 2)),
+        "x_s": dma((outer, inner, 2)),
+        "x_r": dma((outer, inner, 2)),
+        "ahead_s": dma((outer - 1, inner, 2)),
+        "part_s": dma((outer + 1,)),
+        "part_r": dma((outer + 1,)),
+        "pair_s": dma((outer + 1, n_tp // 2)),
+        "pair_r": dma((outer + 1, n_tp // 2)),
+        "hid_s": dma((outer + 1,)),
+        "hid_r": dma((outer + 1,)),
         "ret_s": dma((outer, inner)),
         "ret_r": dma((n_sp,)),
-        "over_s": dma((outer, inner, 2)),
-        "over_r": dma((2, 2, inner, 2)),
-        "sum_s": dma((2, 2)),
-        "far_r": dma((2,)),
+        "beside": vmem((outer - 1, inner, rw, width), BF16),
+        "beside_s": dma((outer - 1, inner, CUTS)),
+        "beside_r": dma((outer - 1, inner, CUTS)),
+        "ret_h": dma((inner, CUTS)),
+        "over_s": dma((outer, inner, CUTS)),
+        "over_r": dma((2, 2, inner, CUTS)),
+        "sum_s": dma((2, CUTS)),
+        "far_r": dma((CUTS,)),
     }
 
 

time: 85 us -> 80.3 us (0.945)
  Pallas kernels: 83.2 us -> 78.5 us
    pallas_call x1, Pallas kernels: 83.2 us -> 78.5 us  [layer(): pl.pallas_call(functools.partial(layer_kernel, n_sp, n_tp, inner, el, cap...]
where the time goes in v4:
time: 80.3 us; the launch traced here: 80.1 us
  Pallas kernels  78.5 us (98%)
  local copies, waits for them, and re-layouts  1.67 us (2%)
    pallas_call x1, Pallas kernels, layer(): pl.pallas_call(functools.partial(layer_kernel, n_sp, n_tp, inner, el, cap...  78.5 us
    unnamed x1, local copies, waits for them, and re-layouts  1.67 us

profile of v4, /device:TPU:0, one launch (start us, length us, event | category | flops | bytes accessed | tf_op | source)
XLA Modules:
  0.0 80.1 jit_solution(5085607820185630477)
XLA Ops:
  0.0 78.5 %shard_map.145 = bf16[128,1024]{1,0:T(8,128)(2,1)} custom-call(bf16[128,512]{1,0:T(8,128)(2,1)} %refs_0_.1, bf16[128,512]{1,0:T(8,128)(2,1)} %refs_1_.1, bf16[128,512]{1,0:T(8,128)(2,1)} %refs_2_.1, bf16[4,128]{1,0:T(4,128)(2,1)} %bitcast.5, bf16[128,1024]{1,0:T(8,128)(2,1)} %refs_4_.1, bf16[2048,1024]{1,0:T(8,128)(2,1)} %refs_5_.1, f32[1,1024]{1,0:T(1,128)} %bitcast.4, ...), custom_call_target="tpu_custom_call" | custom-call | flops 10000000000 | bytes 16777216 | tf_op jit(solution)/shard_map/pallas_call | solution.py:1368
  78.5 1.7 %copy.17 = bf16[128,1024]{1,0:T(8,128)(2,1)} copy(bf16[128,1024]{1,0:T(8,128)(2,1)} %shard_map.145) | data formatting | bytes 524288

commit v5 on v4

--- a/solution.py
+++ b/solution.py
@@ -925,7 +925,7 @@
         for c in self.own_copies():
             c.start()
         self.wait_route()
-        self.middle_only(lambda: self.push(0, 0))
+        self.middle_only(lambda: self.push(0, 0), lambda: self.push(0, 1))
         self.send_squares()
         self.select(0)
         self.middle_only(lambda: self.relay(0), lambda: self.pass_on(1, 0))
@@ -941,7 +941,6 @@
         self.middle_only(
             lambda: self.pass_on(2, 0),
             lambda: self.pass_on(2, 1),
-            lambda: self.push(0, 1),
             lambda: self.select(2),
             lambda: self.select(3),
         )
@@ -955,8 +954,8 @@
         self.hidden(1)
         self.pair(2)
         self.gate_up(3)
+        self.pair(3)
         self.down_rows(1)
-        self.pair(3)
         self.hidden(2)
         self.end_only(lambda: self.bring_along(1))
         self.down_rows(2)

time: 80.3 us -> 79.6 us (level)
  no operation moved by 1% of the time
where the time goes in v5:
time: 79.6 us; the launch traced here: 79.5 us
  Pallas kernels  77.8 us (98%)
  local copies, waits for them, and re-layouts  1.67 us (2%)
    pallas_call x1, Pallas kernels, layer(): pl.pallas_call(functools.partial(layer_kernel, n_sp, n_tp, inner, el, cap...  77.8 us
    unnamed x1, local copies, waits for them, and re-layouts  1.67 us

profile of v5, /device:TPU:0, one launch (start us, length us, event | category | flops | bytes accessed | tf_op | source)
XLA Modules:
  0.0 79.5 jit_solution(18222027271904618455)
XLA Ops:
  0.0 77.8 %shard_map.145 = bf16[128,1024]{1,0:T(8,128)(2,1)} custom-call(bf16[128,512]{1,0:T(8,128)(2,1)} %refs_0_.1, bf16[128,512]{1,0:T(8,128)(2,1)} %refs_1_.1, bf16[128,512]{1,0:T(8,128)(2,1)} %refs_2_.1, bf16[4,128]{1,0:T(4,128)(2,1)} %bitcast.5, bf16[128,1024]{1,0:T(8,128)(2,1)} %refs_4_.1, bf16[2048,1024]{1,0:T(8,128)(2,1)} %refs_5_.1, f32[1,1024]{1,0:T(1,128)} %bitcast.4, ...), custom_call_target="tpu_custom_call" | custom-call | flops 10000000000 | bytes 16777216 | tf_op jit(solution)/shard_map/pallas_call | solution.py:1367
  77.8 1.7 %copy.17 = bf16[128,1024]{1,0:T(8,128)(2,1)} copy(bf16[128,1024]{1,0:T(8,128)(2,1)} %shard_map.145) | data formatting | bytes 524288
